TPU v7x, 512 devices: a whole 4x8x8 slice. The times are simulated.
512 devices in a mesh: sp: 32 (over z, x), tp: 16 (over y, core).
Axes of the slice: x: 4, y: 8, z: 8, core: 2. Of those that a mesh axis runs over, the one named last changes fastest.
Arguments:
- query_one: bfloat16 [8192, 1024], P('sp', 'tp'), may hold values from -6 to 6
- key_one: bfloat16 [8192, 1024], P('sp', 'tp'), may hold values from -6 to 6
- value_one: bfloat16 [8192, 2048], P('sp', 'tp'), may hold values from -6 to 6
- gate_one: bfloat16 [8192, 2048], P('sp', 'tp'), may hold values from -6 to 6
- decay_one: float32 [2, 8192, 1024], P(None, 'sp', 'tp')
- query_two: bfloat16 [8192, 2048], P('sp', 'tp'), may hold values from -6 to 6
- key_two: bfloat16 [8192, 2048], P('sp', 'tp'), may hold values from -6 to 6
- value_two: bfloat16 [8192, 2048], P('sp', 'tp'), may hold values from -6 to 6
- gate_two: bfloat16 [8192, 2048], P('sp', 'tp'), may hold values from -6 to 6
- decay_two: float32 [2, 8192, 2048], P(None, 'sp', 'tp')
- head_gain: float32 [128], replicated, may hold values from 0.1 to 1.9
- proj_one: bfloat16 [2048, 2048], P('tp'), may hold values from -0.09375 to 0.09375
- proj_two: bfloat16 [2048, 2048], P('tp'), may hold values from -0.09375 to 0.09375
- stream: bfloat16 [8192, 2048], P('sp'), may hold values from -6 to 6
- gain_mix: float32 [2048], replicated, may hold values from 0.1 to 1.9
- gain_moe: float32 [2048], replicated, may hold values from 0.1 to 1.9
- routes: int32 [8192, 2], P('sp'), may hold values from 0 to 31, all different within a row; in each aligned block of 256 rows (0 to 255, 256 to 511, ...) at most 24 rows name the same one
- affinity: float32 [8192, 2], P('sp'), may hold values from 0.1 to 1
- expert_gate: bfloat16 [32, 2048, 2048], P('sp', None, 'tp'), may hold values from -0.125 to 0.125
- expert_up: bfloat16 [32, 2048, 2048], P('sp', None, 'tp'), may hold values from -0.125 to 0.125
- expert_down: bfloat16 [32, 2048, 2048], P('sp', 'tp'), may hold values from -0.125 to 0.125
Outputs:
- output: bfloat16 [8192, 2048], P(('sp', 'tp'))
Inputs may be any that keep to these rules, and one draw needn't show every extreme that they name: `routes`: in the 256 rows of one index of sp no expert is named more than 24 times, a bound that some block reaches there in every draw; a row names 2 different experts.
All inputs are finite; a program needn't handle non-finite values.
Results may differ from a plain program's by a relative error of at most 0.017.
Values may be sent and summed in bfloat16 or wider, within the bound.
A program may use at most 64 MiB of HBM per device.

v0:
```python
import functools

import jax
import jax.numpy as jnp
from jax import lax
from jax.experimental import pallas as pl
from jax.experimental.pallas import tpu as pltpu
from jax.sharding import PartitionSpec as P

DK_A = 64
DK_B = 128
BLK = 64
SHARPNESS = 16.0
F32 = jnp.float32
BF16 = jnp.bfloat16
MESH = pl.DeviceIdType.MESH
VMEM = pl.BlockSpec(memory_space=pltpu.VMEM)
DMA = pltpu.SemaphoreType.DMA


def params(collective_id=None):
    if collective_id is None:
        return pltpu.CompilerParams(vmem_limit_bytes=48 * 2**20)
    return pltpu.CompilerParams(
        vmem_limit_bytes=48 * 2**20, collective_id=collective_id, has_side_effects=True
    )


def mm(a, b):
    return jnp.dot(a, b, preferred_element_type=F32)


def mm_nt(a, b):
    return lax.dot_general(a, b, (((1,), (1,)), ((), ())), preferred_element_type=F32)


def mm_tn(a, b):
    return lax.dot_general(a, b, (((0,), (0,)), ((), ())), preferred_element_type=F32)


def log_sigmoid(x):
    return jnp.minimum(x, 0.0) - jnp.log1p(jnp.exp(-jnp.abs(x)))


def silu(x):
    return x / (1.0 + jnp.exp(-x))


def layer_norm(values, gain):
    mean = jnp.mean(values, axis=-1, keepdims=True)
    spread = jnp.mean(jnp.square(values - mean), axis=-1, keepdims=True)
    return (values - mean) * lax.rsqrt(spread + 1e-05) * gain


def greet(peers):
    barrier = pltpu.get_barrier_semaphore()
    for peer in peers:
        pl.semaphore_signal(barrier, inc=1, device_id=peer, device_id_type=MESH)
    pl.semaphore_wait(barrier, len(peers))


def remote(src, dst, send, recv, peer):
    return pltpu.make_async_remote_copy(
        src_ref=src, dst_ref=dst, send_sem=send, recv_sem=recv, device_id=peer, device_id_type=MESH
    )


def across(me, k, n):
    place, bit = 0, 1
    while bit < n:
        digit = lax.rem(me // bit, 2)
        place = place + (1 - digit if k & bit else digit) * bit
        bit *= 2
    return place


def state_kernel(ka, va, da, kb, vb, db, stack, cum):
    rows = ka.shape[0]
    count = rows // BLK
    ii = lax.broadcasted_iota(jnp.int32, (rows, rows), 0)
    jj = lax.broadcasted_iota(jnp.int32, (rows, rows), 1)
    same = (ii // BLK) == (jj // BLK)
    lower = jnp.where(same & (ii >= jj), 1.0, 0.0).astype(BF16)
    upper = jnp.where(same & (ii <= jj), 1.0, 0.0).astype(BF16)
    base = 0
    for k, v, d, dk in ((ka, va, da, DK_A), (kb, vb, db, DK_B)):
        wide = k.shape[1]
        heads = wide // dk
        dv = v.shape[1] // heads
        keys = k[...].astype(F32)
        for way in range(2):
            fade = log_sigmoid(d[way]) / SHARPNESS
            high = fade.astype(BF16)
            low = (fade - high.astype(F32)).astype(BF16)
            tri = lower if way == 0 else upper
            total = mm(tri, high) + mm(tri, low)
            cum[way, :, base : base + wide] = total
            tail = jnp.zeros((1, wide), F32)
            weighted = [None] * count
            for b in reversed(range(count)) if way == 0 else range(count):
                part = total[b * BLK : (b + 1) * BLK]
                last = part[BLK - 1 : BLK] if way == 0 else part[0:1]
                weighted[b] = (keys[b * BLK : (b + 1) * BLK] * jnp.exp(last - part + tail)).astype(BF16)
                tail = tail + last
            weighted = jnp.concatenate(weighted, axis=0)
            states = [
                mm_tn(v[:, h * dv : (h + 1) * dv], weighted[:, h * dk : (h + 1) * dk]).astype(BF16)
                for h in range(heads)
            ]
            states = states[0] if heads == 1 else jnp.concatenate(states, axis=1)
            thigh = tail.astype(BF16).astype(F32)
            row = lax.broadcasted_iota(jnp.int32, (16, wide), 0)
            fades = jnp.where(row == 0, thigh, jnp.where(row == 1, tail - thigh, 0.0)).astype(BF16)
            half = dv // 2
            for i in range(2):
                stack[i, way, 0:half, base : base + wide] = states[i * half : (i + 1) * half]
                stack[i, way, half : half + 16, base : base + wide] = fades
        base += wide


def spread(total, wide):
    row = lax.broadcasted_iota(jnp.int32, (16, wide), 0)
    high = total.astype(BF16).astype(F32)
    return jnp.where(row == 0, high, jnp.where(row == 1, total - high, 0.0)).astype(BF16)


def states_exchange_kernel(n, stack, out, xbox, agg, zbox, outbox, xs, xr, zs, zr, bs, br):
    me = lax.axis_index("sp")
    side = lax.rem(me, 2)
    pair = me // 2
    pairs = n // 2
    partner = me + 1 - 2 * side
    half = out.shape[2]
    lanes = out.shape[3]
    chunk = 256 if lanes % 256 == 0 else lanes
    count = lanes // chunk

    def pair_at(j):
        return lax.rem(pair + j, pairs)

    greet([{"sp": partner}] + [{"sp": pair_at(j) * 2 + side} for j in range(1, pairs)])

    def at(c):
        return pl.ds(c * chunk, chunk)

    def swap(c):
        return remote(
            stack.at[1 - side, :, :, at(c)], xbox.at[:, :, at(c)], xs.at[c], xr.at[c], {"sp": partner}
        )

    def along(c, j):
        way = jnp.where(pair_at(j) < pair, 1, 0)
        return remote(
            agg.at[way, :, at(c)], zbox.at[pair, :, at(c)], zs.at[c, j], zr.at[c, j],
            {"sp": pair_at(j) * 2 + side},
        )

    def back(c):
        return remote(
            outbox.at[:, :, at(c)], out.at[:, side, :, at(c)], bs.at[c], br.at[c], {"sp": partner}
        )

    for c in range(count):
        swap(c).start()
    zbox[pair] = jnp.zeros_like(zbox[pair])

    def load(ref, index, c):
        block = ref[index + (slice(None), at(c))].astype(F32)
        return block[0:half], block[half : half + 1] + block[half + 1 : half + 2]

    def both(c, way):
        own, own_fade = load(stack, (side, way), c)
        other, other_fade = load(xbox, (way,), c)
        low = side == 0
        return (
            jnp.where(low, own, other), jnp.where(low, own_fade, other_fade),
            jnp.where(low, other, own), jnp.where(low, other_fade, own_fade),
        )

    for c in range(count):
        swap(c).wait_recv()
        s0, t0, s1, t1 = both(c, 0)
        agg[0, 0:half, at(c)] = (jnp.exp(t1) * s0 + s1).astype(BF16)
        agg[0, half : half + 16, at(c)] = spread(t0 + t1, chunk)
        s0, t0, s1, t1 = both(c, 1)
        agg[1, 0:half, at(c)] = (jnp.exp(t0) * s1 + s0).astype(BF16)
        agg[1, half : half + 16, at(c)] = spread(t0 + t1, chunk)
        for j in range(1, pairs):
            along(c, j).start()
    for c in range(count):
        for j in range(1, pairs):
            along(c, j).wait_recv()
        ahead = jnp.zeros((half, chunk), F32)
        behind = jnp.zeros((half, chunk), F32)
        for s in range(pairs):
            state, fade = load(zbox, (s,), c)
            ahead = jnp.where(s < pair, jnp.exp(fade) * ahead + state, ahead)
        for s in reversed(range(pairs)):
            state, fade = load(zbox, (s,), c)
            behind = jnp.where(s > pair, jnp.exp(fade) * behind + state, behind)
        low = side == 0
        s0, t0, _, _ = both(c, 0)
        next_ahead = jnp.exp(t0) * ahead + s0
        _, _, s1, t1 = both(c, 1)
        next_behind = jnp.exp(t1) * behind + s1
        outbox[0, :, at(c)] = jnp.where(low, next_ahead, ahead).astype(BF16)
        outbox[1, :, at(c)] = jnp.where(low, behind, next_behind).astype(BF16)
        back(c).start()
        out[0, side, :, at(c)] = jnp.where(low, ahead, next_ahead).astype(BF16)
        out[1, side, :, at(c)] = jnp.where(low, next_behind, behind).astype(BF16)
    for c in range(count):
        swap(c).wait_send()
        for j in range(1, pairs):
            along(c, j).wait_send()
        back(c).wait_send()
        remote(
            outbox.at[:, :, at(c)], out.at[:, 1 - side, :, at(c)], bs.at[c], br.at[c], {"sp": partner}
        ).wait_recv()


def mix_kernel(states, cum, qa, ka, va, ga, qb, kb, vb, gb, gain, pa, pb, out, heads_ref):
    rows = qa.shape[0]
    count = rows // BLK
    dv = gain.shape[1]
    ii = lax.broadcasted_iota(jnp.int32, (BLK, BLK), 0)
    jj = lax.broadcasted_iota(jnp.int32, (BLK, BLK), 1)
    base = 0
    column = 0
    for q, k, v, g, dk in ((qa, ka, va, ga, DK_A), (qb, kb, vb, gb, DK_B)):
        heads = q.shape[1] // dk
        for h in range(heads):
            lanes = slice(base + h * dk, base + (h + 1) * dk)
            own = slice(h * dk, (h + 1) * dk)
            vown = slice(h * dv, (h + 1) * dv)
            forward = jnp.concatenate([states[0, i, :, lanes] for i in range(2)], axis=0).astype(F32)
            backward = jnp.concatenate([states[1, i, :, lanes] for i in range(2)], axis=0).astype(F32)
            mixed = [None] * count
            readers = [None] * count
            growth = [None] * count
            for b in range(count):
                at = slice(b * BLK, (b + 1) * BLK)
                query = q[at, own].astype(F32) * dk ** (-0.5)
                key = k[at, own].astype(F32)
                value = v[at, vown]
                cf = cum[0, at, lanes]
                cb = cum[1, at, lanes]
                qf = (query * jnp.exp(cf)).astype(BF16)
                kf = (key * jnp.exp(-cf)).astype(BF16)
                qr = (query * jnp.exp(cb)).astype(BF16)
                kr = (key * jnp.exp(-cb)).astype(BF16)
                scores = jnp.where(ii >= jj, mm_nt(qf, kf), 0.0) + jnp.where(ii <= jj, mm_nt(qr, kr), 0.0)
                inner = mm(scores.astype(BF16), value)
                lastf = cf[BLK - 1 : BLK]
                inner = inner + mm_nt(qf, forward.astype(BF16))
                if b < count - 1:
                    kfs = (key * jnp.exp(lastf - cf)).astype(BF16)
                    forward = jnp.exp(lastf) * forward + mm_tn(value, kfs)
                mixed[b] = inner
                readers[b] = qr
                lastb = cb[0:1]
                if b > 0:
                    kbs = (key * jnp.exp(lastb - cb)).astype(BF16)
                    growth[b] = (jnp.exp(lastb), mm_tn(value, kbs))
            for b in reversed(range(count)):
                at = slice(b * BLK, (b + 1) * BLK)
                whole = mixed[b] + mm_nt(readers[b], backward.astype(BF16))
                if b > 0:
                    backward = growth[b][0] * backward + growth[b][1]
                scale = lax.rsqrt(jnp.mean(whole * whole, axis=-1, keepdims=True) + 1e-06)
                heads_ref[at, column + h * dv : column + (h + 1) * dv] = (
                    whole * scale * gain[...] * silu(g[at, vown].astype(F32))
                ).astype(BF16)
        base += heads * dk
        column += heads * dv
    split = pa.shape[0]
    width = out.shape[1]
    tile = min(512, width)
    for j in range(width // tile):
        cols = slice(j * tile, (j + 1) * tile)
        out[:, cols] = (
            mm(heads_ref[:, :split], pa[:, cols]) + mm(heads_ref[:, split:], pb[:, cols])
        ).astype(BF16)


def settle_kernel(
    n, part, stream, gain, settled, columns, inbox, mid, midbox, outbox, cs, cr, ys, yr, send2, recv2
):
    me = lax.axis_index("tp")
    own = part.shape[0] // n
    wide = part.shape[1] // n
    core = lax.rem(me, 2)
    line = me // 2
    lines = n // 2
    greet([{"tp": lax.rem(me + k, n)} for k in range(1, n)])

    def rows_of(i):
        return pl.ds(pl.multiple_of(i * own, own), own)

    def cols_of(i):
        return pl.ds(pl.multiple_of(i * wide, wide), wide)

    def line_at(j):
        return lax.rem(line + j, lines)

    def to_core(j):
        i = line_at(j) * 2 + 1 - core
        return remote(
            part.at[rows_of(i), :], inbox.at[j], cs.at[j], cr.at[j], {"tp": me + 1 - 2 * core}
        )

    def to_line(j):
        return remote(mid.at[j], midbox.at[j], ys.at[j], yr.at[j], {"tp": line_at(j) * 2 + core})

    for j in reversed(range(lines)):
        to_core(j).start()
    for j in reversed(range(lines)):
        to_core(j).wait_recv()
        mine = part[rows_of(line_at(j) * 2 + core), :].astype(F32) + inbox[j].astype(F32)
        if j > 0:
            mid[j] = mine.astype(BF16)
            to_line(j).start()
        else:
            total = mine
    for j in range(1, lines):
        to_line(j).wait_recv()
        total = total + midbox[j].astype(F32)
    total = total.astype(BF16).astype(F32)
    value = layer_norm(stream[rows_of(me), :].astype(F32) + total, gain[...])
    settled[...] = value
    outbox[...] = value.astype(BF16)
    second = []
    for k in range(1, n):
        peer = lax.rem(me + k, n)
        copy = remote(
            outbox.at[:, cols_of(peer)], columns.at[rows_of(me), :], send2.at[k], recv2.at[k], {"tp": peer}
        )
        copy.start()
        second.append(copy)
    columns[rows_of(me), :] = outbox[:, cols_of(me)]
    for k in range(1, n):
        source = lax.rem(me + n - k, n)
        second[k - 1].wait_send()
        remote(
            outbox.at[:, cols_of(source)], columns.at[rows_of(source), :], send2.at[k], recv2.at[k], {"tp": source}
        ).wait_recv()
    for j in range(lines):
        to_core(j).wait_send()
        if j > 0:
            to_line(j).wait_send()


def slots_of(routes, capacity, experts):
    rows, top = routes.shape
    lane = lax.broadcasted_iota(jnp.int32, (rows, max(128, experts)), 1)
    hots = [routes[:, i : i + 1] == lane for i in range(top)]
    named = sum(jnp.where(h, 1.0, 0.0) for h in hots)
    ii = lax.broadcasted_iota(jnp.int32, (rows, rows), 0)
    jj = lax.broadcasted_iota(jnp.int32, (rows, rows), 1)
    before = mm(jnp.where(ii > jj, 1.0, 0.0).astype(BF16), named.astype(BF16))
    slots = []
    for i in range(top):
        rank = jnp.sum(jnp.where(hots[i], before, 0.0), axis=1, keepdims=True).astype(jnp.int32)
        slots.append(routes[:, i : i + 1] * capacity + rank)
    return slots


def pick_kernel(capacity, experts, routes, columns, out):
    slots = slots_of(routes[...], capacity, experts)
    rows = columns.shape[0]
    lane = lax.broadcasted_iota(jnp.int32, (rows, experts * capacity), 1)
    hot = sum(jnp.where(lane == s, 1.0, 0.0) for s in slots).astype(BF16)
    out[...] = mm_tn(hot, columns[...]).astype(BF16)


def dispatch_kernel(n, m, x, out, ss, sr, ys, yr, cs, cr, fs, fr, local):
    me = lax.axis_index("sp")
    my = lax.axis_index("tp")
    wide = x.shape[2]
    core = lax.rem(my, 2)
    line = my // 2
    lines = m // 2
    partner = my + 1 - 2 * core

    def cols_of(i):
        return pl.ds(pl.multiple_of(i * wide, wide), wide)

    def line_peer(j):
        return lax.rem(line + j, lines) * 2 + core

    def line_source(j):
        return lax.rem(line + lines - j, lines) * 2 + core

    greet(
        [{"sp": lax.rem(me + k, n)} for k in range(1, n)]
        + [{"tp": partner}]
        + [{"tp": line_peer(j)} for j in range(1, lines)]
    )

    def cross(k):
        peer = across(me, k, n)
        return remote(x.at[peer], out.at[me, :, cols_of(my)], ss.at[k], sr.at[k], {"sp": peer})

    for k in range(1, n):
        cross(k).start()
    own = pltpu.make_async_copy(x.at[me], out.at[me, :, cols_of(my)], local)
    own.start()

    def block(s, i):
        return out.at[s, :, cols_of(i)]

    def to_line(k, s, j, i):
        return remote(block(s, i), block(s, i), ys.at[k, j], yr.at[k, j], {"tp": line_peer(j)})

    def to_core(k, s, i):
        return remote(block(s, i), block(s, i), cs.at[k], cr.at[k], {"tp": partner})

    def forward(k, s, j, i):
        return remote(block(s, i), block(s, i), fs.at[k, j], fr.at[k, j], {"tp": partner})

    def source(k):
        return across(me, k, n)

    def hand_on(k, s):
        for j in range(1, lines):
            to_line(k, s, j, my).start()
        to_core(k, s, my).start()

    def pass_on(k, s):
        for j in range(1, lines):
            i = line_source(j)
            to_line(k, s, j, i).wait_recv()
            forward(k, s, j, i).start()

    own.wait()
    hand_on(0, me)
    for k in range(1, n):
        s = source(k)
        remote(x.at[0], block(s, my), ss.at[k], sr.at[k], {"sp": s}).wait_recv()
        hand_on(k, s)
        pass_on(k - 1, source(k - 1))
    pass_on(n - 1, source(n - 1))
    for k in range(n):
        s = source(k)
        if k > 0:
            cross(k).wait_send()
        to_core(k, s, my).wait_send()
        to_core(k, s, partner).wait_recv()
        for j in range(1, lines):
            i = line_source(j)
            to_line(k, s, j, my).wait_send()
            forward(k, s, j, i).wait_send()
            forward(k, s, j, i + 1 - 2 * core).wait_recv()


def return_kernel(n, m, x, out, inbox, mid, midbox, last, cs, cr, ys, yr, ss, sr):
    me = lax.axis_index("sp")
    my = lax.axis_index("tp")
    wide = out.shape[2]
    core = lax.rem(my, 2)
    line = my // 2
    lines = m // 2
    partner = my + 1 - 2 * core

    def cols_of(i):
        return pl.ds(pl.multiple_of(i * wide, wide), wide)

    def line_at(j):
        return lax.rem(line + j, lines)

    greet(
        [{"sp": lax.rem(me + k, n)} for k in range(1, n)]
        + [{"tp": partner}]
        + [{"tp": line_at(j) * 2 + core} for j in range(1, lines)]
    )

    def place(k):
        return across(me, n - 1 - k, n)

    def to_core(k, j):
        i = line_at(j) * 2 + 1 - core
        return remote(x.at[place(k), :, cols_of(i)], inbox.at[k, j], cs.at[k, j], cr.at[k, j], {"tp": partner})

    def to_line(k, j):
        return remote(
            mid.at[k, j], midbox.at[k, j], ys.at[k, j], yr.at[k, j], {"tp": line_at(j) * 2 + core}
        )

    def cross(k):
        peer = place(k)
        return remote(last.at[k], out.at[me], ss.at[k], sr.at[k], {"sp": peer})

    for k in range(n):
        for j in reversed(range(lines)):
            to_core(k, j).start()

    def first(k):
        for j in reversed(range(lines)):
            to_core(k, j).wait_recv()
            i = line_at(j) * 2 + core
            mine = x[place(k), :, cols_of(i)].astype(F32) + inbox[k, j].astype(F32)
            mid[k, j] = mine.astype(BF16)
            if j > 0:
                to_line(k, j).start()

    def second(k):
        total = mid[k, 0].astype(F32)
        for j in range(1, lines):
            to_line(k, j).wait_recv()
            total = total + midbox[k, j].astype(F32)
        if k < n - 1:
            last[k] = total.astype(BF16)
            cross(k).start()
        else:
            out[me] = total.astype(BF16)

    first(0)
    for k in range(1, n):
        first(k)
        second(k - 1)
    second(n - 1)
    for k in range(n):
        for j in range(lines):
            to_core(k, j).wait_send()
            if j > 0:
                to_line(k, j).wait_send()
        if k < n - 1:
            cross(k).wait_send()
            s = place(k)
            remote(last.at[k], out.at[s], ss.at[k], sr.at[k], {"sp": s}).wait_recv()


def finish_kernel(n, capacity, experts, routes, affinity, pieces, settled, gain, out, term, mixture, send, recv):
    me = lax.axis_index("tp")
    rows = routes.shape[0]
    own = rows // n
    wide = pieces.shape[1]
    greet([{"tp": lax.rem(me + k, n)} for k in range(1, n)])

    def rows_of(i):
        return pl.ds(pl.multiple_of(i * own, own), own)

    def cols_of(i):
        return pl.ds(pl.multiple_of(i * wide, wide), wide)

    slots = slots_of(routes[...], capacity, experts)
    weights = affinity[...] / jnp.sum(affinity[...], axis=-1, keepdims=True)
    lane = lax.broadcasted_iota(jnp.int32, (rows, experts * capacity), 1)
    total = jnp.zeros((rows, wide), F32)
    for i, slot in enumerate(slots):
        hot = jnp.where(lane == slot, 1.0, 0.0).astype(BF16)
        total = total + weights[:, i : i + 1] * mm(hot, pieces[...])
    term[...] = total.astype(BF16)
    copies = []
    for k in range(1, n):
        peer = lax.rem(me + k, n)
        copy = remote(term.at[rows_of(peer), :], mixture.at[:, cols_of(me)], send.at[k], recv.at[k], {"tp": peer})
        copy.start()
        copies.append(copy)
    mixture[:, cols_of(me)] = term[rows_of(me), :]
    for k in range(1, n):
        source = lax.rem(me + n - k, n)
        copies[k - 1].wait_send()
        remote(
            term.at[rows_of(source), :], mixture.at[:, cols_of(source)], send.at[k], recv.at[k], {"tp": source}
        ).wait_recv()
    out[...] = layer_norm(settled[...] + mixture[...].astype(F32), gain[...]).astype(BF16)


def call(kernel, outs, scratch, count, collective_id=None):
    single = not isinstance(outs, list)
    return pl.pallas_call(
        kernel,
        out_shape=outs,
        in_specs=[VMEM] * count,
        out_specs=VMEM if single else [VMEM] * len(outs),
        scratch_shapes=scratch,
        compiler_params=params(collective_id),
    )


def body(
    query_one,
    key_one,
    value_one,
    gate_one,
    decay_one,
    query_two,
    key_two,
    value_two,
    gate_two,
    decay_two,
    head_gain,
    proj_one,
    proj_two,
    stream,
    gain_mix,
    gain_moe,
    routes,
    affinity,
    expert_gate,
    expert_up,
    expert_down,
):
    shape = jax.ShapeDtypeStruct
    rows = query_one.shape[0]
    n = lax.axis_size("sp")
    m = lax.axis_size("tp")
    width = stream.shape[1]
    own = rows // m
    wide = width // m
    dv = head_gain.shape[0]
    lanes = query_one.shape[1] + query_two.shape[1]
    values = value_one.shape[1] + value_two.shape[1]
    local_experts = expert_gate.shape[0]
    experts = local_experts * n
    top = routes.shape[1]
    capacity = 3 * rows * top // (2 * experts)
    room = local_experts * capacity

    half = dv // 2
    stack, cum = call(
        state_kernel, [shape((2, 2, half + 16, lanes), BF16), shape((2, rows, lanes), F32)], [], 6
    )(key_one, value_one, decay_one, key_two, value_two, decay_two)
    chunks = max(1, lanes // 256)
    states = call(
        functools.partial(states_exchange_kernel, n),
        shape((2, 2, half, lanes), BF16),
        [
            pltpu.VMEM((2, half + 16, lanes), BF16),
            pltpu.VMEM((2, half + 16, lanes), BF16),
            pltpu.VMEM((n // 2, half + 16, lanes), BF16),
            pltpu.VMEM((2, half, lanes), BF16),
            DMA((chunks,)), DMA((chunks,)), DMA((chunks, n // 2)), DMA((chunks, n // 2)),
            DMA((chunks,)), DMA((chunks,)),
        ],
        1,
        1,
    )(stack)
    part = call(mix_kernel, shape((rows, width), BF16), [pltpu.VMEM((rows, values), BF16)], 13)(
        states, cum, query_one, key_one, value_one, gate_one, query_two, key_two, value_two, gate_two,
        head_gain.reshape(1, -1), proj_one, proj_two,
    )
    settled, columns = call(
        functools.partial(settle_kernel, m),
        [shape((own, width), F32), shape((rows, wide), BF16)],
        [pltpu.VMEM((m // 2, own, width), BF16)] * 3
        + [pltpu.VMEM((own, width), BF16)]
        + [DMA((m // 2,))] * 4
        + [DMA((m,))] * 2,
        3,
        2,
    )(part, stream, gain_mix.reshape(1, -1))
    outgoing = call(
        functools.partial(pick_kernel, capacity, experts), shape((experts * capacity, wide), BF16), [], 2
    )(routes, columns)
    lines = m // 2
    received = call(
        functools.partial(dispatch_kernel, n, m),
        shape((n, room, width), BF16),
        [DMA((n,)), DMA((n,)), DMA((n, lines)), DMA((n, lines)), DMA((n,)), DMA((n,)),
         DMA((n, lines)), DMA((n, lines)), DMA],
        1,
        3,
    )(outgoing.reshape(n, room, wide))
    x = received.reshape(n, local_experts, capacity, width)
    results = []
    for e in range(local_experts):
        xe = x[:, e].reshape(n * capacity, width)
        gate = mm(xe, expert_gate[e])
        upward = mm(xe, expert_up[e])
        act = (jax.nn.silu(gate) * upward).astype(BF16)
        results.append(mm(act, expert_down[e]).astype(BF16).reshape(n, capacity, width))
    partial_value = results[0] if local_experts == 1 else jnp.concatenate(results, axis=1)
    pieces = call(
        functools.partial(return_kernel, n, m),
        shape((n, room, wide), BF16),
        [pltpu.VMEM((n, lines, room, wide), BF16)] * 3
        + [pltpu.VMEM((n, room, wide), BF16)]
        + [DMA((n, lines))] * 4
        + [DMA((n,))] * 2,
        1,
        4,
    )(partial_value)
    return call(
        functools.partial(finish_kernel, m, capacity, experts),
        shape((own, width), BF16),
        [pltpu.VMEM((rows, wide), BF16), pltpu.VMEM((own, width), BF16), DMA((m,)), DMA((m,))],
        5,
        5,
    )(routes, affinity, pieces.reshape(experts * capacity, wide), settled, gain_moe.reshape(1, -1))


def solution(mesh):
    return jax.shard_map(
        body,
        mesh=mesh,
        in_specs=(
            P("sp", "tp"),
            P("sp", "tp"),
            P("sp", "tp"),
            P("sp", "tp"),
            P(None, "sp", "tp"),
            P("sp", "tp"),
            P("sp", "tp"),
            P("sp", "tp"),
            P("sp", "tp"),
            P(None, "sp", "tp"),
            P(),
            P("tp", None),
            P("tp", None),
            P("sp", None),
            P(),
            P(),
            P("sp", None),
            P("sp", None),
            P("sp", None, "tp"),
            P("sp", None, "tp"),
            P("sp", "tp", None),
        ),
        out_specs=P(("sp", "tp"), None),
        check_vma=False,
    )
```

profile of v0, /device:TPU:1, one launch (start us, length us, event | category | flops | bytes accessed | tf_op | source)
XLA Modules:
  0.0 309.2 jit_solution(14422741724002826274)
XLA Ops:
  0.0 0.0 copy-start
  0.0 1.0 copy.22.ka
  1.0 1.0 copy.23.da
  2.0 0.0 copy-start.6
  2.0 0.9 copy-done.6
  3.0 0.0 copy-start.7
  3.0 0.8 copy-done.7
  3.8 0.0 copy-start.9
  3.8 0.8 copy-done.9
  4.7 0.0 copy-start.11
  4.7 0.8 copy-done.11
  5.5 1.4 shard_map.199
  6.9 33.0 %shard_map.200.states = bf16[2,2,64,192]{3,2,1,0:T(8,128)(2,1)S(1)} custom-call(bf16[2,2,80,192]{3,2,1,0:T(8,128)(2,1)S(1)} %get-tuple-element.9.stack), custom_call_target="tpu_custom_call" | custom-call | tf_op jit(solution)/shard_map/pallas_call | solution.py:625
  39.9 0.9 copy.24.qa
  40.8 0.0 copy-start.4
  40.8 1.0 copy-done.4
  41.9 1.0 copy-done.5
  42.9 0.8 copy-done.8
  43.7 0.8 copy-done.10
  44.6 0.8 copy-done.12
  45.4 0.8 copy-done.13
  46.3 0.8 copy-done.14
  47.1 0.8 copy-done.15
  47.9 0.7 copy-done.18
  48.6 2.5 shard_map.201.part
  51.1 0.0 copy-start.19
  51.1 0.0 copy-done.3
  51.2 0.0 copy-done.16
  51.2 30.4 %shard_map.202 = (f32[16,2048]{1,0:T(8,128)S(1)}, bf16[256,128]{1,0:T(8,128)(2,1)S(1)}) custom-call(bf16[256,2048]{1,0:T(8,128)(2,1)S(1)} %shard_map.201.part, bf16[256,2048]{1,0:T(8,128)(2,1)S(1)} %copy-done.3, f32[1,2048]{1,0:T(1,128)S(1)} %bitcast.24), custom_call_target="tpu_custom_call" | custom-call | tf_op jit(solution)/shard_map/pallas_call | solution.py:643
  81.6 0.0 copy-done.21
  81.6 0.1 copy.27.routes
  81.7 0.9 shard_map.203
  82.6 103.0 %shard_map.204 = bf16[32,24,2048]{2,1,0:T(8,128)(2,1)S(1)} custom-call(bf16[32,24,128]{2,1,0:T(8,128)(2,1)S(1)} %bitcast.22), custom_call_target="tpu_custom_call" | custom-call | tf_op jit(solution)/shard_map/pallas_call | solution.py:657
  185.6 0.0 copy-start.1
  185.6 0.0 copy-start.20
  185.6 1.6 copy-done.1
  187.2 0.0 copy-done.19
  187.2 1.0 fusion.4
  188.2 0.0 copy-done
  188.2 0.0 copy-done.20
  188.2 6.9 %convolution_convert_fusion = bf16[768,2048]{1,0:T(8,128)(2,1)} fusion(bf16[768,2048]{1,0:T(8,128)(2,1)} %bitcast.20, bf16[1,128,2048]{2,1,0:T(8,128)(2,1)S(1)} %copy-done, bf16[1,2048,128]{2,1,0:T(8,128)(2,1)S(1)} %copy-done.20, f32[768,128]{1,0:T(8,128)S(1)} %fusion.4), kind=kOutput, calls=%fused_computation | convolution fusion | flops 807469056 | bytes 7733248 | tf_op jit(solution)/shard_map/dot_general | solution.py:30
  195.2 1.9 copy-done.2
  197.0 87.4 %shard_map.205 = bf16[32,24,128]{2,1,0:T(8,128)(2,1)S(1)} custom-call(bf16[32,24,2048]{2,1,0:T(8,128)(2,1)S(1)} %bitcast.21), custom_call_target="tpu_custom_call" | custom-call | tf_op jit(solution)/shard_map/pallas_call | solution.py:674
  284.4 0.0 copy-done.22
  284.4 0.1 copy.28.affinity
  284.6 0.0 copy-done.17
  284.6 23.9 %shard_map.206 = bf16[16,2048]{1,0:T(8,128)(2,1)S(1)} custom-call(s32[256,2]{1,0:T(8,128)S(1)} %copy.27.routes, f32[256,2]{1,0:T(8,128)S(1)} %copy.28.affinity, bf16[768,128]{1,0:T(8,128)(2,1)S(1)} %bitcast.23, f32[16,2048]{1,0:T(8,128)S(1)} %get-tuple-element.12.settled, f32[1,2048]{1,0:T(1,128)S(1)} %bitcast.25), custom_call_target="tpu_custom_call" | custom-call | tf_op jit(solution)/shard_map/pallas_call | solution.py:684
  308.5 0.6 copy.30
  (14 shorter events, 0.0 us)
Async XLA Ops:
  0.0 188.2 %copy-start = (bf16[1,128,2048]{2,1,0:T(8,128)(2,1)S(1)}, bf16[1,128,2048]{2,1,0:T(8,128)(2,1)}, u32[]{:S(2)}) copy-start(bf16[1,128,2048]{2,1,0:T(8,128)(2,1)} %param.41) | copy-start | bytes 1572868
  0.0 51.1 %copy-start.3 = (bf16[256,2048]{1,0:T(8,128)(2,1)S(1)}, bf16[256,2048]{1,0:T(8,128)(2,1)}, u32[]{:S(2)}) copy-start(bf16[256,2048]{1,0:T(8,128)(2,1)} %stream.1) | copy-start | bytes 3145732
  2.0 1.0 copy-start.6
  3.0 0.8 copy-start.7
  3.8 0.8 copy-start.9
  4.7 0.8 copy-start.11
  5.5 45.6 %copy-start.16 = (f32[2048]{0:T(1024)S(1)}, f32[2048]{0:T(1024)}, u32[]{:S(2)}) copy-start(f32[2048]{0:T(1024)} %param.35) | copy-start | bytes 24580
  5.5 76.1 %copy-start.21 = (s32[256,2]{0,1:T(2,128)S(1)}, s32[256,2]{0,1:T(2,128)}, u32[]{:S(2)}) copy-start(s32[256,2]{0,1:T(2,128)} %param.37) | copy-start | bytes 6148
  40.8 1.0 copy-start.4
  41.9 1.0 copy-start.5
  42.9 0.8 copy-start.8
  43.7 0.8 copy-start.10
  44.6 0.8 copy-start.12
  45.4 0.8 copy-start.13
  46.3 0.8 copy-start.14
  47.1 0.8 copy-start.15
  47.9 0.7 copy-start.18
  51.1 136.1 %copy-start.19 = (bf16[1,2048,128]{2,1,0:T(8,128)(2,1)S(1)}, bf16[1,2048,128]{2,1,0:T(8,128)(2,1)}, u32[]{:S(2)}) copy-start(bf16[1,2048,128]{2,1,0:T(8,128)(2,1)} %param.39) | copy-start | bytes 1572868
  185.6 1.6 copy-start.1
  185.6 2.6 copy-start.20
  195.1 1.9 copy-start.2
  197.0 87.4 %copy-start.22 = (f32[256,2]{0,1:T(2,128)S(1)}, f32[256,2]{0,1:T(2,128)}, u32[]{:S(2)}) copy-start(f32[256,2]{0,1:T(2,128)} %param.38) | copy-start | bytes 6148
  197.0 87.5 %copy-start.17 = (f32[2048]{0:T(1024)S(1)}, f32[2048]{0:T(1024)}, u32[]{:S(2)}) copy-start(f32[2048]{0:T(1024)} %param.36) | copy-start | bytes 24580
where the time goes:
time: 310 us; the launch traced here: 309 us
  Pallas kernels  283 us (91%)
  local copies, waits for them, and re-layouts  18.6 us (6%)
  matrix products  7.88 us (3%)
    pallas_call x1, Pallas kernels, body(): call(functools.partial(dispatch_kernel, n, m), shape((n, room, width), BF...  103 us
    pallas_call x1, Pallas kernels, body(): call(functools.partial(return_kernel, n, m), shape((n, room, wide), BF16)...  87.4 us
    pallas_call x1, Pallas kernels, body(): call(functools.partial(states_exchange_kernel, n), shape((2, 2, half, lan...  33 us
    pallas_call x1, Pallas kernels, body(): call(functools.partial(settle_kernel, m), [shape((own, width), F32), shap...  30.4 us
    pallas_call x1, Pallas kernels, body(): call(functools.partial(finish_kernel, m, capacity, experts), shape((own,...  23.9 us
    unnamed x52, local copies, waits for them, and re-layouts  18.6 us
    dot_general x2, matrix products, mm(): return jnp.dot(a, b, preferred_element_type=F32)  7.88 us

commit v1 on v0

--- a/solution.py
+++ b/solution.py
@@ -11,6 +11,7 @@
 DK_B = 128
 BLK = 64
 SHARPNESS = 16.0
+ZN, XN, YN = 8, 4, 8
 F32 = jnp.float32
 BF16 = jnp.bfloat16
 MESH = pl.DeviceIdType.MESH
@@ -349,221 +350,332 @@
             to_line(j).wait_send()
 
 
-def slots_of(routes, capacity, experts):
-    rows, top = routes.shape
-    lane = lax.broadcasted_iota(jnp.int32, (rows, max(128, experts)), 1)
-    hots = [routes[:, i : i + 1] == lane for i in range(top)]
+def ring_sites():
+    sp = lax.axis_index("sp")
+    tp = lax.axis_index("tp")
+    return sp, sp // XN, lax.rem(sp, XN), tp, tp // 2, lax.rem(tp, 2)
+
+
+def sp_at(z, x, dz, dx):
+    return lax.rem(z + dz, ZN) * XN + lax.rem(x + dx, XN)
+
+
+def near(d, n):
+    return min(d, n - d)
+
+
+def carried(way, d, k):
+    return d < YN // 2 or k == way
+
+
+def moe_kernel(
+    routes, affinity, columns, settled, gain, wg_hbm, wu_hbm, wd_hbm, out,
+    wg, wu, wd, mixhi, mixlo, picked, x, acc, act, p, s, r, q, pieces, term, mixture,
+    wls, wrs, wrr, as_, ar, gs, gr, rs, rr, bs, br, fs, fr,
+):
+    sp, z, xx, tp, y, c = ring_sites()
+    n = ZN * XN
+    m = YN * 2
+    half = YN // 2
+    per = XN // 2
+    slots = picked.shape[1]
+    count = ZN * per
+    group = count * slots
+    lanes = picked.shape[2]
+    rows = columns.shape[0]
+    own = rows // m
+    partner = {"tp": tp + 1 - 2 * c}
+
+    barrier = pltpu.get_barrier_semaphore()
+
+    def greet_one(peer):
+        pl.semaphore_signal(barrier, inc=1, device_id=peer, device_id_type=MESH)
+
+    for k in range(1, m):
+        greet_one({"tp": lax.rem(tp + k, m)})
+    for dz in range(ZN):
+        for dx in range(XN):
+            if dz or dx:
+                greet_one({"sp": sp_at(z, xx, dz, dx), "tp": y * 2 + dx % 2})
+    for j in range(count):
+        peer = {"sp": sp_at(z, xx, j // per, 2 * (j % per) + c), "tp": y * 2 + 1 - c}
+        if j == 0:
+            pl.when(c == 1)(functools.partial(greet_one, peer))
+        else:
+            greet_one(peer)
+
+    loads = [
+        pltpu.make_async_copy(src.at[0], dst.at[0], wls.at[i])
+        for i, (src, dst) in enumerate(((wg_hbm, wg), (wu_hbm, wu), (wd_hbm, wd)))
+    ]
+    for load in loads:
+        load.start()
+
+    lane = lax.broadcasted_iota(jnp.int32, (n, rows), 0)
+    hots = [routes[i : i + 1, :] == lane for i in range(2)]
     named = sum(jnp.where(h, 1.0, 0.0) for h in hots)
     ii = lax.broadcasted_iota(jnp.int32, (rows, rows), 0)
     jj = lax.broadcasted_iota(jnp.int32, (rows, rows), 1)
-    before = mm(jnp.where(ii > jj, 1.0, 0.0).astype(BF16), named.astype(BF16))
-    slots = []
-    for i in range(top):
-        rank = jnp.sum(jnp.where(hots[i], before, 0.0), axis=1, keepdims=True).astype(jnp.int32)
-        slots.append(routes[:, i : i + 1] * capacity + rank)
-    return slots
-
-
-def pick_kernel(capacity, experts, routes, columns, out):
-    slots = slots_of(routes[...], capacity, experts)
-    rows = columns.shape[0]
-    lane = lax.broadcasted_iota(jnp.int32, (rows, experts * capacity), 1)
-    hot = sum(jnp.where(lane == s, 1.0, 0.0) for s in slots).astype(BF16)
-    out[...] = mm_tn(hot, columns[...]).astype(BF16)
-
-
-def dispatch_kernel(n, m, x, out, ss, sr, ys, yr, cs, cr, fs, fr, local):
-    me = lax.axis_index("sp")
-    my = lax.axis_index("tp")
-    wide = x.shape[2]
-    core = lax.rem(my, 2)
-    line = my // 2
-    lines = m // 2
-    partner = my + 1 - 2 * core
-
-    def cols_of(i):
-        return pl.ds(pl.multiple_of(i * wide, wide), wide)
-
-    def line_peer(j):
-        return lax.rem(line + j, lines) * 2 + core
-
-    def line_source(j):
-        return lax.rem(line + lines - j, lines) * 2 + core
-
-    greet(
-        [{"sp": lax.rem(me + k, n)} for k in range(1, n)]
-        + [{"tp": partner}]
-        + [{"tp": line_peer(j)} for j in range(1, lines)]
+    before = mm(named.astype(BF16), jnp.where(ii < jj, 1.0, 0.0).astype(BF16))
+    place = [
+        routes[i : i + 1, :] * slots
+        + jnp.sum(jnp.where(hots[i], before, 0.0), axis=0, keepdims=True).astype(jnp.int32)
+        for i in range(2)
+    ]
+    seat = lax.broadcasted_iota(jnp.int32, (n * slots, rows), 0)
+    hot = jnp.where((seat == place[0]) | (seat == place[1]), 1.0, 0.0).astype(BF16)
+    picked[...] = mm(hot, columns[...]).astype(BF16).reshape(picked.shape)
+
+    pl.semaphore_wait(barrier, (m - 1) + (n - 1) + (count - 1) + c)
+
+    def dispatch(dz, dx):
+        e = sp_at(z, xx, dz, dx)
+        rz, rx = (-dz) % ZN, (-dx) % XN
+        j = rz * per + rx // 2
+        return remote(
+            picked.at[e], x.at[y, c, j], as_.at[dz * XN + dx], ar.at[c, j], {"sp": e, "tp": y * 2 + dx % 2}
+        )
+
+    home = pltpu.make_async_copy(picked.at[sp], x.at[y, 0, 0], ar.at[0, 0])
+    offsets = sorted(
+        [(dz, dx) for dz in range(ZN) for dx in range(XN)],
+        key=lambda o: -(near(o[0], ZN) + near(o[1], XN)),
     )
-
-    def cross(k):
-        peer = across(me, k, n)
-        return remote(x.at[peer], out.at[me, :, cols_of(my)], ss.at[k], sr.at[k], {"sp": peer})
-
-    for k in range(1, n):
-        cross(k).start()
-    own = pltpu.make_async_copy(x.at[me], out.at[me, :, cols_of(my)], local)
-    own.start()
-
-    def block(s, i):
-        return out.at[s, :, cols_of(i)]
-
-    def to_line(k, s, j, i):
-        return remote(block(s, i), block(s, i), ys.at[k, j], yr.at[k, j], {"tp": line_peer(j)})
-
-    def to_core(k, s, i):
-        return remote(block(s, i), block(s, i), cs.at[k], cr.at[k], {"tp": partner})
-
-    def forward(k, s, j, i):
-        return remote(block(s, i), block(s, i), fs.at[k, j], fr.at[k, j], {"tp": partner})
-
-    def source(k):
-        return across(me, k, n)
-
-    def hand_on(k, s):
-        for j in range(1, lines):
-            to_line(k, s, j, my).start()
-        to_core(k, s, my).start()
-
-    def pass_on(k, s):
-        for j in range(1, lines):
-            i = line_source(j)
-            to_line(k, s, j, i).wait_recv()
-            forward(k, s, j, i).start()
-
-    own.wait()
-    hand_on(0, me)
-    for k in range(1, n):
-        s = source(k)
-        remote(x.at[0], block(s, my), ss.at[k], sr.at[k], {"sp": s}).wait_recv()
-        hand_on(k, s)
-        pass_on(k - 1, source(k - 1))
-    pass_on(n - 1, source(n - 1))
-    for k in range(n):
-        s = source(k)
-        if k > 0:
-            cross(k).wait_send()
-        to_core(k, s, my).wait_send()
-        to_core(k, s, partner).wait_recv()
-        for j in range(1, lines):
-            i = line_source(j)
-            to_line(k, s, j, my).wait_send()
-            forward(k, s, j, i).wait_send()
-            forward(k, s, j, i + 1 - 2 * core).wait_recv()
-
-
-def return_kernel(n, m, x, out, inbox, mid, midbox, last, cs, cr, ys, yr, ss, sr):
-    me = lax.axis_index("sp")
-    my = lax.axis_index("tp")
-    wide = out.shape[2]
-    core = lax.rem(my, 2)
-    line = my // 2
-    lines = m // 2
-    partner = my + 1 - 2 * core
-
-    def cols_of(i):
-        return pl.ds(pl.multiple_of(i * wide, wide), wide)
-
-    def line_at(j):
-        return lax.rem(line + j, lines)
-
-    greet(
-        [{"sp": lax.rem(me + k, n)} for k in range(1, n)]
-        + [{"tp": partner}]
-        + [{"tp": line_at(j) * 2 + core} for j in range(1, lines)]
-    )
-
-    def place(k):
-        return across(me, n - 1 - k, n)
-
-    def to_core(k, j):
-        i = line_at(j) * 2 + 1 - core
-        return remote(x.at[place(k), :, cols_of(i)], inbox.at[k, j], cs.at[k, j], cr.at[k, j], {"tp": partner})
-
-    def to_line(k, j):
+    for dz, dx in offsets:
+        if dz or dx:
+            dispatch(dz, dx).start()
+    pl.when(c == 0)(lambda: home.start())
+    pl.when(c == 1)(lambda: dispatch(0, 0).start())
+
+    swaps = [
+        remote(src.at[0], dst.at[1], wrs.at[i], wrr.at[i], partner)
+        for i, (src, dst) in enumerate(((wg_hbm, wg), (wu_hbm, wu), (wd_hbm, wd)))
+    ]
+    for swap in swaps:
+        swap.start()
+
+    weights = [affinity[i : i + 1, :] / (affinity[0:1, :] + affinity[1:2, :]) for i in range(2)]
+    mix = jnp.where(seat == place[0], weights[0], jnp.where(seat == place[1], weights[1], 0.0)).T
+    high = mix.astype(BF16)
+    mixhi[...] = high
+    mixlo[...] = (mix - high.astype(F32)).astype(BF16)
+
+    def arrive(k, j):
+        remote(picked.at[0], x.at[y, k, j], as_.at[0], ar.at[k, j], partner).wait_recv()
+
+    def hop(way, h, k):
+        step = 1 if way == 0 else YN - 1
+        b = lax.rem(y + (h - 1) * (YN - step), YN)
         return remote(
-            mid.at[k, j], midbox.at[k, j], ys.at[k, j], yr.at[k, j], {"tp": line_at(j) * 2 + core}
-        )
-
-    def cross(k):
-        peer = place(k)
-        return remote(last.at[k], out.at[me], ss.at[k], sr.at[k], {"sp": peer})
-
-    for k in range(n):
-        for j in reversed(range(lines)):
-            to_core(k, j).start()
-
-    def first(k):
-        for j in reversed(range(lines)):
-            to_core(k, j).wait_recv()
-            i = line_at(j) * 2 + core
-            mine = x[place(k), :, cols_of(i)].astype(F32) + inbox[k, j].astype(F32)
-            mid[k, j] = mine.astype(BF16)
-            if j > 0:
-                to_line(k, j).start()
-
-    def second(k):
-        total = mid[k, 0].astype(F32)
-        for j in range(1, lines):
-            to_line(k, j).wait_recv()
-            total = total + midbox[k, j].astype(F32)
-        if k < n - 1:
-            last[k] = total.astype(BF16)
-            cross(k).start()
-        else:
-            out[me] = total.astype(BF16)
-
-    first(0)
-    for k in range(1, n):
-        first(k)
-        second(k - 1)
-    second(n - 1)
-    for k in range(n):
-        for j in range(lines):
-            to_core(k, j).wait_send()
-            if j > 0:
-                to_line(k, j).wait_send()
-        if k < n - 1:
-            cross(k).wait_send()
-            s = place(k)
-            remote(last.at[k], out.at[s], ss.at[k], sr.at[k], {"sp": s}).wait_recv()
-
-
-def finish_kernel(n, capacity, experts, routes, affinity, pieces, settled, gain, out, term, mixture, send, recv):
-    me = lax.axis_index("tp")
-    rows = routes.shape[0]
-    own = rows // n
-    wide = pieces.shape[1]
-    greet([{"tp": lax.rem(me + k, n)} for k in range(1, n)])
+            x.at[b, k], x.at[b, k], gs.at[way, h - 1, k], gr.at[way, h - 1, k],
+            {"tp": lax.rem(y + step, YN) * 2 + c},
+        )
+
+    def landed(way, h, k):
+        step = 1 if way == 0 else YN - 1
+        b = lax.rem(y + h * (YN - step), YN)
+        remote(
+            x.at[b, k], x.at[b, k], gs.at[way, h - 1, k], gr.at[way, h - 1, k],
+            {"tp": lax.rem(y + step, YN) * 2 + c},
+        ).wait_recv()
+
+    def widen(b, first=False):
+        at = pl.ds(pl.multiple_of(b * 2 * lanes, 2 * lanes), 2 * lanes)
+        block = jnp.concatenate([x[b, k].reshape(group, lanes) for k in range(2)], axis=1)
+        w = jnp.concatenate([ref[i, at, :] for ref in (wg, wu) for i in range(2)], axis=1)
+        value = mm(block, w)
+        acc[...] = value if first else acc[...] + value
+
+    for k in range(2):
+        for j in range(count):
+            if k == 0 and j == 0:
+                pl.when(c == 0)(lambda: home.wait())
+                pl.when(c == 1)(lambda: arrive(0, 0))
+            else:
+                arrive(k, j)
+        for way in range(2):
+            if carried(way, 1, k):
+                hop(way, 1, k).start()
+    for load in loads:
+        load.wait()
+    for swap in swaps:
+        swap.wait_recv()
+    widen(y, first=True)
+    for h in range(1, half + 1):
+        for k in range(2):
+            for way in range(2):
+                if carried(way, h, k):
+                    landed(way, h, k)
+                    if h < half and carried(way, h + 1, k):
+                        hop(way, h + 1, k).start()
+        widen(lax.rem(y + YN - h, YN))
+        if h < half:
+            widen(lax.rem(y + h, YN))
+
+    hidden = 2 * lanes
+    act[...] = (silu(acc[:, :hidden]) * acc[:, hidden:]).astype(BF16)
+
+    def narrow(o):
+        b = lax.rem(y + o, YN)
+        at = pl.ds(pl.multiple_of(b * hidden, hidden), hidden)
+        p[o] = mm(act[...], jnp.concatenate([wd[i, :, at] for i in range(2)], axis=0))
+
+    def offset(way, d):
+        return d if way == 0 else YN - d
+
+    def part(o, k):
+        return p[o, :, k * lanes : (k + 1) * lanes]
+
+    def pass_sum(way, d, k):
+        step = 1 if way == 0 else YN - 1
+        return remote(
+            s.at[way, d - 1, k], r.at[way, d - 1, k], rs.at[way, d - 1, k], rr.at[way, d - 1, k],
+            {"tp": lax.rem(y + step, YN) * 2 + c},
+        )
+
+    narrow(half)
+    for way in range(2):
+        s[way, half - 1, way] = part(half, way).astype(BF16)
+        pass_sum(way, half, way).start()
+    for d in range(half - 1, 0, -1):
+        narrow(d)
+        narrow(YN - d)
+        for turn in range(2):
+            for way in range(2):
+                k = 1 - turn if way == 0 else turn
+                total = part(offset(way, d), k)
+                if carried(way, d + 1, k):
+                    pass_sum(way, d + 1, k).wait_recv()
+                    total = total + r[way, d, k].astype(F32)
+                s[way, d - 1, k] = total.astype(BF16)
+                pass_sum(way, d, k).start()
+    narrow(0)
+
+    def give(k, j):
+        rz = j // per
+        rx = 2 * (j % per) + c
+        o = ((-rz) % ZN) * XN + lax.rem(XN - rx, XN)
+        return remote(
+            q.at[k, j], pieces.at[sp], bs.at[k, j], br.at[o], {"sp": sp_at(z, xx, rz, rx), "tp": y * 2 + k}
+        )
+
+    back = pltpu.make_async_copy(q.at[0, 0], pieces.at[sp], br.at[0])
+    for k in range(2):
+        total = part(0, k)
+        for way in range(2):
+            if carried(way, 1, k):
+                pass_sum(way, 1, k).wait_recv()
+                total = total + r[way, 0, k].astype(F32)
+        q[k] = total.astype(BF16).reshape(count, slots, lanes)
+        order = sorted(range(count), key=lambda j: -near(j // per, ZN))
+        for j in order:
+            if k == 0 and j == 0:
+                pl.when(c == 0)(lambda: back.start())
+                pl.when(c == 1)(lambda: give(0, 0).start())
+            else:
+                give(k, j).start()
+
+    for dz in range(ZN):
+        for dx in range(XN):
+            o = dz * XN + dx
+            e = sp_at(z, xx, dz, dx)
+            coming = remote(q.at[0, 0], pieces.at[e], bs.at[0, 0], br.at[o], partner)
+            if o == 0:
+                pl.when(c == 0)(lambda: back.wait())
+                pl.when(c == 1)(lambda: coming.wait_recv())
+            else:
+                coming.wait_recv()
+
+    flat = pieces[...].reshape(n * slots, lanes)
+    term[...] = (mm(mixhi[...], flat) + mm(mixlo[...], flat)).astype(BF16)
 
     def rows_of(i):
         return pl.ds(pl.multiple_of(i * own, own), own)
 
     def cols_of(i):
-        return pl.ds(pl.multiple_of(i * wide, wide), wide)
-
-    slots = slots_of(routes[...], capacity, experts)
-    weights = affinity[...] / jnp.sum(affinity[...], axis=-1, keepdims=True)
-    lane = lax.broadcasted_iota(jnp.int32, (rows, experts * capacity), 1)
-    total = jnp.zeros((rows, wide), F32)
-    for i, slot in enumerate(slots):
-        hot = jnp.where(lane == slot, 1.0, 0.0).astype(BF16)
-        total = total + weights[:, i : i + 1] * mm(hot, pieces[...])
-    term[...] = total.astype(BF16)
-    copies = []
-    for k in range(1, n):
-        peer = lax.rem(me + k, n)
-        copy = remote(term.at[rows_of(peer), :], mixture.at[:, cols_of(me)], send.at[k], recv.at[k], {"tp": peer})
-        copy.start()
-        copies.append(copy)
-    mixture[:, cols_of(me)] = term[rows_of(me), :]
-    for k in range(1, n):
-        source = lax.rem(me + n - k, n)
-        copies[k - 1].wait_send()
+        return pl.ds(pl.multiple_of(i * lanes, lanes), lanes)
+
+    def spread_rows(k):
+        peer = lax.rem(tp + k, m)
+        return remote(term.at[rows_of(peer), :], mixture.at[:, cols_of(tp)], fs.at[k], fr.at[k], {"tp": peer})
+
+    for k in sorted(range(1, m), key=lambda k: -near(k // 2, YN)):
+        spread_rows(k).start()
+    mixture[:, cols_of(tp)] = term[rows_of(tp), :]
+    for k in range(1, m):
+        source = lax.rem(tp + m - k, m)
         remote(
-            term.at[rows_of(source), :], mixture.at[:, cols_of(source)], send.at[k], recv.at[k], {"tp": source}
+            term.at[rows_of(source), :], mixture.at[:, cols_of(source)], fs.at[k], fr.at[k], {"tp": source}
         ).wait_recv()
     out[...] = layer_norm(settled[...] + mixture[...].astype(F32), gain[...]).astype(BF16)
+
+    for dz, dx in offsets:
+        if dz or dx:
+            dispatch(dz, dx).wait_send()
+    pl.when(c == 1)(lambda: dispatch(0, 0).wait_send())
+    for swap in swaps:
+        swap.wait_send()
+    for way in range(2):
+        for d in range(1, half + 1):
+            for k in range(2):
+                if carried(way, d, k):
+                    hop(way, d, k).wait_send()
+                    pass_sum(way, d, k).wait_send()
+    for k in range(2):
+        for j in range(count):
+            if k == 0 and j == 0:
+                pl.when(c == 1)(lambda: give(0, 0).wait_send())
+            else:
+                give(k, j).wait_send()
+    for k in range(1, m):
+        spread_rows(k).wait_send()
+
+
+ANY = pl.BlockSpec(memory_space=pl.ANY)
+
+
+def moe_call(routes, affinity, columns, settled, gain, wg, wu, wd):
+    n = ZN * XN
+    m = YN * 2
+    half = YN // 2
+    rows, lanes = columns.shape
+    slots = 3 * rows * 2 // (2 * n)
+    count = n // 2
+    group = count * slots
+    width = settled.shape[1]
+    own = rows // m
+    scratch = [
+        pltpu.VMEM((2, width, lanes), BF16),
+        pltpu.VMEM((2, width, lanes), BF16),
+        pltpu.VMEM((2, lanes, width), BF16),
+        pltpu.VMEM((rows, n * slots), BF16),
+        pltpu.VMEM((rows, n * slots), BF16),
+        pltpu.VMEM((n, slots, lanes), BF16),
+        pltpu.VMEM((YN, 2, count, slots, lanes), BF16),
+        pltpu.VMEM((group, 4 * lanes), F32),
+        pltpu.VMEM((group, 2 * lanes), BF16),
+        pltpu.VMEM((YN, group, 2 * lanes), F32),
+        pltpu.VMEM((2, half, 2, group, lanes), BF16),
+        pltpu.VMEM((2, half, 2, group, lanes), BF16),
+        pltpu.VMEM((2, count, slots, lanes), BF16),
+        pltpu.VMEM((n, slots, lanes), BF16),
+        pltpu.VMEM((rows, lanes), BF16),
+        pltpu.VMEM((own, width), BF16),
+        DMA((3,)), DMA((3,)), DMA((3,)),
+        DMA((n,)), DMA((2, count)),
+        DMA((2, half, 2)), DMA((2, half, 2)),
+        DMA((2, half, 2)), DMA((2, half, 2)),
+        DMA((2, count)), DMA((n,)),
+        DMA((m,)), DMA((m,)),
+    ]
+    return pl.pallas_call(
+        moe_kernel,
+        out_shape=jax.ShapeDtypeStruct((own, width), BF16),
+        in_specs=[VMEM] * 5 + [ANY] * 3,
+        out_specs=VMEM,
+        scratch_shapes=scratch,
+        compiler_params=params(3),
+    )(routes, affinity, columns, settled, gain, wg, wu, wd)
 
 
 def call(kernel, outs, scratch, count, collective_id=None):
@@ -611,12 +723,6 @@
     dv = head_gain.shape[0]
     lanes = query_one.shape[1] + query_two.shape[1]
     values = value_one.shape[1] + value_two.shape[1]
-    local_experts = expert_gate.shape[0]
-    experts = local_experts * n
-    top = routes.shape[1]
-    capacity = 3 * rows * top // (2 * experts)
-    room = local_experts * capacity
-
     half = dv // 2
     stack, cum = call(
         state_kernel, [shape((2, 2, half + 16, lanes), BF16), shape((2, rows, lanes), F32)], [], 6
@@ -650,44 +756,9 @@
         3,
         2,
     )(part, stream, gain_mix.reshape(1, -1))
-    outgoing = call(
-        functools.partial(pick_kernel, capacity, experts), shape((experts * capacity, wide), BF16), [], 2
-    )(routes, columns)
-    lines = m // 2
-    received = call(
-        functools.partial(dispatch_kernel, n, m),
-        shape((n, room, width), BF16),
-        [DMA((n,)), DMA((n,)), DMA((n, lines)), DMA((n, lines)), DMA((n,)), DMA((n,)),
-         DMA((n, lines)), DMA((n, lines)), DMA],
-        1,
-        3,
-    )(outgoing.reshape(n, room, wide))
-    x = received.reshape(n, local_experts, capacity, width)
-    results = []
-    for e in range(local_experts):
-        xe = x[:, e].reshape(n * capacity, width)
-        gate = mm(xe, expert_gate[e])
-        upward = mm(xe, expert_up[e])
-        act = (jax.nn.silu(gate) * upward).astype(BF16)
-        results.append(mm(act, expert_down[e]).astype(BF16).reshape(n, capacity, width))
-    partial_value = results[0] if local_experts == 1 else jnp.concatenate(results, axis=1)
-    pieces = call(
-        functools.partial(return_kernel, n, m),
-        shape((n, room, wide), BF16),
-        [pltpu.VMEM((n, lines, room, wide), BF16)] * 3
-        + [pltpu.VMEM((n, room, wide), BF16)]
-        + [DMA((n, lines))] * 4
-        + [DMA((n,))] * 2,
-        1,
-        4,
-    )(partial_value)
-    return call(
-        functools.partial(finish_kernel, m, capacity, experts),
-        shape((own, width), BF16),
-        [pltpu.VMEM((rows, wide), BF16), pltpu.VMEM((own, width), BF16), DMA((m,)), DMA((m,))],
-        5,
-        5,
-    )(routes, affinity, pieces.reshape(experts * capacity, wide), settled, gain_moe.reshape(1, -1))
+    return moe_call(
+        routes.T, affinity.T, columns, settled, gain_moe.reshape(1, -1), expert_gate, expert_up, expert_down
+    )
 
 
 def solution(mesh):

time: 310 us -> 140 us (0.45)
  Pallas kernels: 283 us -> 136 us
  local copies, waits for them, and re-layouts: 18.6 us -> 4.28 us
  matrix products: 7.88 us -> 0 us
    pallas_call x4 -> x1, Pallas kernels: 215 us -> 68.1 us  [moe_call(): pl.pallas_call(moe_kernel, out_shape=jax.ShapeDtypeStruct((own, width), B...]
    unnamed x52 -> x42, local copies, waits for them, and re-layouts: 18.6 us -> 4.28 us
    dot_general x2 -> x0, matrix products: 7.88 us -> none  [mm(): return jnp.dot(a, b, preferred_element_type=F32)]
where the time goes in v1:
time: 140 us
  Pallas kernels  136 us (97%)
  local copies, waits for them, and re-layouts  4.28 us (3%)
    pallas_call x1, Pallas kernels, moe_call(): pl.pallas_call(moe_kernel, out_shape=jax.ShapeDtypeStruct((own, width), B...  68.1 us
    pallas_call x1, Pallas kernels, body(): call(functools.partial(states_exchange_kernel, n), shape((2, 2, half, lan...  33.1 us
    pallas_call x1, Pallas kernels, body(): call(functools.partial(settle_kernel, m), [shape((own, width), F32), shap...  30.4 us
    unnamed x42, local copies, waits for them, and re-layouts  4.28 us

profile of v1, /device:TPU:1, one launch (start us, length us, event | category | flops | bytes accessed | tf_op | source)
XLA Modules:
  0.0 140.2 jit_solution(17794537797990693228)
XLA Ops:
  0.0 0.0 copy-start.18
  0.0 0.0 copy-start.11
  0.0 0.9 copy.22.ka
  0.9 0.0 copy-done.18
  0.9 0.0 copy-start.6
  0.9 0.1 copy.24.qa
  1.0 0.0 copy-start.7
  1.1 0.0 copy-start.8
  1.1 0.0 copy-start.9
  1.1 0.0 copy-start.10
  1.1 1.1 copy.23.da
  2.2 0.0 copy-done.6
  2.2 0.0 copy-done.7
  2.2 0.0 copy-done.8
  2.2 0.0 copy-done.9
  2.2 0.0 copy-start.4
  2.2 0.0 copy-start.5
  2.2 1.4 shard_map.199
  3.7 0.0 copy-start.17
  3.7 33.1 %shard_map.200.states = bf16[2,2,64,192]{3,2,1,0:T(8,128)(2,1)S(1)} custom-call(bf16[2,2,80,192]{3,2,1,0:T(8,128)(2,1)S(1)} %get-tuple-element.9.stack), custom_call_target="tpu_custom_call" | custom-call | tf_op jit(solution)/shard_map/pallas_call | solution.py:731
  36.8 0.0 copy-done.11
  36.8 0.0 copy-done.10
  36.8 0.0 copy-done.4
  36.8 0.0 copy-done.5
  36.8 0.0 copy-done.17
  36.9 0.0 copy-start.12
  36.9 0.8 copy-done.12
  37.7 0.0 copy-start
  37.7 0.0 copy-start.13
  37.7 2.6 %shard_map.201.part = bf16[256,2048]{1,0:T(8,128)(2,1)S(1)} custom-call(bf16[2,2,64,192]{3,2,1,0:T(8,128)(2,1)S(1)} %shard_map.200.states, f32[2,256,192]{2,1,0:T(8,128)S(1)} %get-tuple-element.10.cum, bf16[256,64]{1,0:T(8,128)(2,1)S(1)} %copy.24.qa, bf16[256,64]{1,0:T(8,128)(2,1)S(1)} %copy.22.ka, bf16[256,128]{1,0:T(8,128)(2,1)S(1)} %copy-done.7, ...), custom_call_target="tpu_custom_call" | custom-call | tf_op jit(solution)/shard_map/pallas_call | solution.py:745
  40.3 0.0 copy-done
  40.3 0.0 copy-done.13
  40.3 0.0 copy-start.1
  40.3 0.0 copy-start.2
  40.3 0.0 copy-start.3
  40.3 0.0 copy-start.14
  40.3 0.0 copy-start.16
  40.3 30.4 %shard_map.202 = (f32[16,2048]{1,0:T(8,128)S(1)}, bf16[256,128]{1,0:T(8,128)(2,1)S(1)}) custom-call(bf16[256,2048]{1,0:T(8,128)(2,1)S(1)} %shard_map.201.part, bf16[256,2048]{1,0:T(8,128)(2,1)S(1)} %copy-done, f32[1,2048]{1,0:T(1,128)S(1)} %bitcast.5), custom_call_target="tpu_custom_call" | custom-call | tf_op jit(solution)/shard_map/pallas_call | solution.py:749
  70.8 0.0 copy-start.15
  70.8 0.0 copy-done.1
  70.8 0.0 copy-done.2
  70.8 0.0 copy-done.3
  70.8 0.0 copy-done.14
  70.8 0.0 copy-done.16
  70.8 0.6 copy-done.15
  71.4 68.1 %shard_map.203 = bf16[16,2048]{1,0:T(8,128)(2,1)S(1)} custom-call(s32[2,256]{1,0:T(2,128)S(1)} %bitcast.7, f32[2,256]{1,0:T(2,128)S(1)} %bitcast.8, bf16[256,128]{1,0:T(8,128)(2,1)S(1)} %get-tuple-element.11.columns, f32[16,2048]{1,0:T(8,128)S(1)} %get-tuple-element.12.settled, f32[1,2048]{1,0:T(1,128)S(1)} %bitcast.6, bf16[1,2048,128]{2,1,0:T(8,128)(2,1)S(1)} %copy-done.1, ...), custom_call_target="tpu_custom_call" | custom-call | tf_op jit(solution)/shard_map/pallas_call | solution.py:671
  139.6 0.6 copy.27
Async XLA Ops:
  0.0 0.9 copy-start.18
  0.0 36.8 %copy-start.11 = (bf16[256,128]{1,0:T(8,128)(2,1)S(1)}, bf16[256,128]{1,0:T(8,128)(2,1)}, u32[]{:S(2)}) copy-start(bf16[256,128]{1,0:T(8,128)(2,1)} %qb.1) | copy-start | bytes 196612
  0.9 1.3 copy-start.6
  1.0 1.1 copy-start.7
  1.1 1.1 copy-start.8
  1.1 1.1 copy-start.9
  1.1 35.7 %copy-start.10 = (bf16[256,128]{1,0:T(8,128)(2,1)S(1)}, bf16[256,128]{1,0:T(8,128)(2,1)}, u32[]{:S(2)}) copy-start(bf16[256,128]{1,0:T(8,128)(2,1)} %ga.1) | copy-start | bytes 196612
  2.2 34.6 %copy-start.4 = (bf16[128,2048]{1,0:T(8,128)(2,1)S(1)}, bf16[128,2048]{1,0:T(8,128)(2,1)}, u32[]{:S(2)}) copy-start(bf16[128,2048]{1,0:T(8,128)(2,1)} %pa.1) | copy-start | bytes 1572868
  2.2 34.6 %copy-start.5 = (bf16[128,2048]{1,0:T(8,128)(2,1)S(1)}, bf16[128,2048]{1,0:T(8,128)(2,1)}, u32[]{:S(2)}) copy-start(bf16[128,2048]{1,0:T(8,128)(2,1)} %pb.1) | copy-start | bytes 1572868
  3.7 33.2 %copy-start.17 = (f32[128]{0:T(128)S(1)}, f32[128]{0:T(128)}, u32[]{:S(2)}) copy-start(f32[128]{0:T(128)} %param.31) | copy-start | bytes 1540
  36.9 0.8 copy-start.12
  37.7 2.6 %copy-start = (bf16[256,2048]{1,0:T(8,128)(2,1)S(1)}, bf16[256,2048]{1,0:T(8,128)(2,1)}, u32[]{:S(2)}) copy-start(bf16[256,2048]{1,0:T(8,128)(2,1)} %stream.1) | copy-start | bytes 3145732
  37.7 2.6 %copy-start.13 = (f32[2048]{0:T(1024)S(1)}, f32[2048]{0:T(1024)}, u32[]{:S(2)}) copy-start(f32[2048]{0:T(1024)} %param.35) | copy-start | bytes 24580
  40.3 30.5 %copy-start.1 = (bf16[1,2048,128]{2,1,0:T(8,128)(2,1)S(1)}, bf16[1,2048,128]{2,1,0:T(8,128)(2,1)}, u32[]{:S(2)}) copy-start(bf16[1,2048,128]{2,1,0:T(8,128)(2,1)} %wg_hbm.1) | copy-start | bytes 1572868
  40.3 30.5 %copy-start.2 = (bf16[1,2048,128]{2,1,0:T(8,128)(2,1)S(1)}, bf16[1,2048,128]{2,1,0:T(8,128)(2,1)}, u32[]{:S(2)}) copy-start(bf16[1,2048,128]{2,1,0:T(8,128)(2,1)} %wu_hbm.1) | copy-start | bytes 1572868
  40.3 30.5 %copy-start.3 = (bf16[1,128,2048]{2,1,0:T(8,128)(2,1)S(1)}, bf16[1,128,2048]{2,1,0:T(8,128)(2,1)}, u32[]{:S(2)}) copy-start(bf16[1,128,2048]{2,1,0:T(8,128)(2,1)} %wd_hbm.1) | copy-start | bytes 1572868
  40.3 30.5 %copy-start.14 = (f32[2048]{0:T(1024)S(1)}, f32[2048]{0:T(1024)}, u32[]{:S(2)}) copy-start(f32[2048]{0:T(1024)} %param.36) | copy-start | bytes 24580
  40.3 30.5 %copy-start.16 = (f32[256,2]{0,1:T(2,128)S(1)}, f32[256,2]{0,1:T(2,128)}, u32[]{:S(2)}) copy-start(f32[256,2]{0,1:T(2,128)} %param.38) | copy-start | bytes 6148
  70.8 0.7 copy-start.15

commit v2 on v1

v2 whole, which is shorter than its diff:
```python
import functools

import jax
import jax.numpy as jnp
from jax import lax
from jax.experimental import pallas as pl
from jax.experimental.pallas import tpu as pltpu
from jax.sharding import PartitionSpec as P

DK_A = 64
DK_B = 128
BLK = 64
SHARPNESS = 16.0
ZN, XN, YN = 8, 4, 8
CUTS = 4
FADES = 8
F32 = jnp.float32
BF16 = jnp.bfloat16
MESH = pl.DeviceIdType.MESH
VMEM = pl.BlockSpec(memory_space=pltpu.VMEM)
ANY = pl.BlockSpec(memory_space=pl.ANY)
DMA = pltpu.SemaphoreType.DMA


def mm(a, b):
    return jnp.dot(a, b, preferred_element_type=F32)


def mm_nt(a, b):
    return lax.dot_general(a, b, (((1,), (1,)), ((), ())), preferred_element_type=F32)


def mm_tn(a, b):
    return lax.dot_general(a, b, (((0,), (0,)), ((), ())), preferred_element_type=F32)


def log_sigmoid(x):
    return jnp.minimum(x, 0.0) - jnp.log1p(jnp.exp(-jnp.abs(x)))


def silu(x):
    return x / (1.0 + jnp.exp(-x))


def layer_norm(values, gain):
    mean = jnp.mean(values, axis=-1, keepdims=True)
    spread = jnp.mean(jnp.square(values - mean), axis=-1, keepdims=True)
    return (values - mean) * lax.rsqrt(spread + 1e-05) * gain


def remote(src, dst, send, recv, peer):
    return pltpu.make_async_remote_copy(
        src_ref=src, dst_ref=dst, send_sem=send, recv_sem=recv, device_id=peer, device_id_type=MESH
    )


def sp_at(z, x, dz, dx):
    return lax.rem(z + dz, ZN) * XN + lax.rem(x + dx, XN)


def near(d, n):
    return min(d, n - d)


def carried(way, d, k, cuts):
    return d < YN // 2 or k // (cuts // 2) == way


def step_of(way):
    return 1 if way == 0 else YN - 1


def fade_rows(total):
    wide = total.shape[1]
    row = lax.broadcasted_iota(jnp.int32, (FADES, wide), 0)
    high = total.astype(BF16).astype(F32)
    return jnp.where(row == 0, high, jnp.where(row == 1, total - high, 0.0)).astype(BF16)


def local_states(keys, values, decays, base, stack, cum):
    rows, wide = keys.shape
    count = rows // BLK
    dv = values.shape[1]
    piece = dv // XN
    ii = lax.broadcasted_iota(jnp.int32, (rows, rows), 0)
    jj = lax.broadcasted_iota(jnp.int32, (rows, rows), 1)
    same = (ii // BLK) == (jj // BLK)
    for way in range(2):
        tri = jnp.where(same & ((ii >= jj) if way == 0 else (ii <= jj)), 1.0, 0.0).astype(BF16)
        fade = log_sigmoid(decays[way]) / SHARPNESS
        high = fade.astype(BF16)
        low = (fade - high.astype(F32)).astype(BF16)
        total = mm(tri, high) + mm(tri, low)
        cum[way, :, base : base + wide] = total
        tail = jnp.zeros((1, wide), F32)
        weighted = [None] * count
        for b in reversed(range(count)) if way == 0 else range(count):
            part = total[b * BLK : (b + 1) * BLK]
            last = part[BLK - 1 : BLK] if way == 0 else part[0:1]
            weighted[b] = (keys[b * BLK : (b + 1) * BLK] * jnp.exp(last - part + tail)).astype(BF16)
            tail = tail + last
        state = mm_tn(values, jnp.concatenate(weighted, axis=0)).astype(BF16)
        fades = fade_rows(tail)
        for i in range(XN):
            stack[i, way, 0:piece, base : base + wide] = state[i * piece : (i + 1) * piece]
            stack[i, way, piece : piece + FADES, base : base + wide] = fades


def local_mix(query, keys, values, base, cum, reach, column, mixed):
    rows, dk = keys.shape
    count = rows // BLK
    dv = values.shape[1]
    ii = lax.broadcasted_iota(jnp.int32, (BLK, BLK), 0)
    jj = lax.broadcasted_iota(jnp.int32, (BLK, BLK), 1)
    lanes = slice(base, base + dk)
    query = query * dk ** (-0.5)
    inner = [None] * count
    readers = [None] * count
    state = None
    passed = jnp.zeros((1, dk), F32)
    for b in range(count):
        at = slice(b * BLK, (b + 1) * BLK)
        value = values[at]
        cf = cum[0, at, lanes]
        cb = cum[1, at, lanes]
        qf = (query[at] * jnp.exp(cf)).astype(BF16)
        kf = (keys[at] * jnp.exp(-cf)).astype(BF16)
        qr = (query[at] * jnp.exp(cb)).astype(BF16)
        kr = (keys[at] * jnp.exp(-cb)).astype(BF16)
        scores = jnp.where(ii >= jj, mm_nt(qf, kf), 0.0) + jnp.where(ii <= jj, mm_nt(qr, kr), 0.0)
        inner[b] = mm(scores.astype(BF16), value)
        if b > 0:
            inner[b] = inner[b] + mm_nt(qf, state.astype(BF16))
        reach[0, at, lanes] = (query[at] * jnp.exp(cf + passed)).astype(BF16)
        last = cf[BLK - 1 : BLK]
        if b < count - 1:
            gain = mm_tn(value, (keys[at] * jnp.exp(last - cf)).astype(BF16))
            state = gain if b == 0 else jnp.exp(last) * state + gain
        passed = passed + last
        readers[b] = qr
    state = None
    passed = jnp.zeros((1, dk), F32)
    for b in reversed(range(count)):
        at = slice(b * BLK, (b + 1) * BLK)
        cb = cum[1, at, lanes]
        if b < count - 1:
            inner[b] = inner[b] + mm_nt(readers[b], state.astype(BF16))
        reach[1, at, lanes] = (query[at] * jnp.exp(cb + passed)).astype(BF16)
        last = cb[0:1]
        if b > 0:
            gain = mm_tn(values[at], (keys[at] * jnp.exp(last - cb)).astype(BF16))
            state = gain if b == count - 1 else jnp.exp(last) * state + gain
        passed = passed + last
        mixed[at, column : column + dv] = inner[b]


def ring_sum(y, c, cuts, part, prepare, s, r, ss, sr, finish):
    half = YN // 2

    def pass_sum(way, d, k):
        return remote(
            s.at[way, d - 1, k], r.at[way, d - 1, k], ss.at[way, d - 1, k], sr.at[way, d - 1, k],
            {"tp": lax.rem(y + step_of(way), YN) * 2 + c},
        )

    def order(way):
        mine = [k for k in range(cuts) if k // (cuts // 2) == way]
        return mine, [k for k in range(cuts) if k not in mine]

    def send(way, d, k):
        total = part(d if way == 0 else YN - d, k)
        if d < half and carried(way, d + 1, k, cuts):
            pass_sum(way, d + 1, k).wait_recv()
            total = total + r[way, d, k].astype(F32)
        s[way, d - 1, k] = total.astype(BF16)
        pass_sum(way, d, k).start()

    prepare(half)
    for turn in range(cuts // 2):
        for way in range(2):
            send(way, half, order(way)[0][turn])
    for d in range(half - 1, 0, -1):
        prepare(d)
        prepare(YN - d)
        for turn in range(cuts):
            for way in range(2):
                near_first, late = order(way)
                ks = late + near_first if d == half - 1 else near_first + late
                if d < half - 1 and half > 2:
                    ks = late + near_first
                send(way, d, ks[turn])
    prepare(0)
    for turn in range(cuts):
        k = (cuts // 2 * (turn % 2) + turn // 2) % cuts
        total = part(0, k)
        for way in range(2):
            if carried(way, 1, k, cuts):
                pass_sum(way, 1, k).wait_recv()
                total = total + r[way, 0, k].astype(F32)
        finish(k, total)

    def settle_sends():
        for way in range(2):
            for d in range(1, half + 1):
                for k in range(cuts):
                    if carried(way, d, k, cuts):
                        pass_sum(way, d, k).wait_send()

    return settle_sends


INPUTS = (
    "qa", "ka", "va", "ga", "da", "qb", "kb", "vb", "gb", "db", "head_gain", "pa", "pb", "stream",
    "gain_mix", "gain_moe", "routes", "affinity", "wg", "wu", "wd",
)


def shapes_of(rows, dv, width):
    n = ZN * XN
    m = YN * 2
    half = YN // 2
    own = rows // m
    lanes = width // m
    slots = 3 * rows * 2 // (2 * n)
    count = n // 2
    group = count * slots
    keys = DK_A + DK_B
    piece = dv // XN
    big = piece + FADES
    mine = rows // 2
    cut = width // CUTS
    v = pltpu.VMEM
    return dict(
        qa=v((DK_A, rows), BF16), ka=v((DK_A, rows), BF16), va=v((rows, dv), BF16), ga=v((rows, dv), BF16),
        da=v((2, DK_A, rows), F32), qb=v((rows, DK_B), BF16), kb=v((rows, DK_B), BF16), vb=v((rows, dv), BF16),
        gb=v((rows, dv), BF16), db=v((2, rows, DK_B), F32), head_gain=v((1, dv), F32),
        stream=v((own, width), BF16), gain_mix=v((1, width), F32), gain_moe=v((1, width), F32),
        routes=v((2, rows), jnp.int32), affinity=v((2, rows), F32),
        pj=v((2, 2, dv, width), BF16), wg=v((2, width, lanes), BF16), wu=v((2, width, lanes), BF16),
        wd=v((2, lanes, width), BF16), early=DMA((19,)), loads=DMA((3,)), swap_s=DMA((5,)), swap_r=DMA((5,)),
        cum=v((2, rows, keys), F32), stack=v((XN, 2, big, keys), BF16), xbox=v((XN, 2, big, keys), BF16),
        agg=v((2, big, keys), BF16), zbox=v((ZN, big, keys), BF16), outx=v((XN, 2, piece, keys), BF16),
        states=v((XN, 2, piece, keys), BF16), xs=DMA((XN,)), xr=DMA((XN,)), zs=DMA((ZN,)), zr=DMA((ZN,)),
        es=DMA((XN,)), er=DMA((XN,)),
        mixed=v((rows, 2 * dv), F32), reach=v((2, rows, keys), BF16), heads=v((2, mine, 2 * dv), BF16),
        hbox=v((mine, 2 * dv), BF16), hs=DMA((2,)), pp=v((YN, own, width), F32),
        s1=v((2, half, CUTS, own, cut), BF16), r1=v((2, half, CUTS, own, cut), BF16),
        s1s=DMA((2, half, CUTS)), s1r=DMA((2, half, CUTS)), settled=v((own, width), F32),
        moe_in=v((own, width), BF16), columns=v((rows, lanes), BF16), cs=DMA((m,)), cr=DMA((m,)),
        hot=v((n * slots, rows), BF16),
        mixhi=v((rows, n * slots), BF16), mixlo=v((rows, n * slots), BF16), picked=v((n, slots, lanes), BF16),
        x=v((YN, 2, count, slots, lanes), BF16), acc=v((group, 4 * lanes), F32), act=v((group, 2 * lanes), BF16),
        p=v((YN, group, 2 * lanes), F32), s2=v((2, half, 2, group, lanes), BF16),
        r2=v((2, half, 2, group, lanes), BF16), s2s=DMA((2, half, 2)), s2r=DMA((2, half, 2)),
        q=v((2, count, slots, lanes), BF16), pieces=v((n, slots, lanes), BF16), term=v((rows, lanes), BF16),
        mixture=v((own, width), BF16), ds=DMA((n,)), dr=DMA((2, count)), gs=DMA((2, half, 2)), gr=DMA((2, half, 2)),
        bs=DMA((2, count)), br=DMA((n,)), fs=DMA((m,)), fr=DMA((m,)),
    )


def layer_kernel(scratch_names, *refs):
    hbm = dict(zip(INPUTS, refs))
    out = refs[len(INPUTS)]
    v = dict(zip(scratch_names, refs[len(INPUTS) + 1 :]))
    sp = lax.axis_index("sp")
    tp = lax.axis_index("tp")
    z, xx, y, c = sp // XN, lax.rem(sp, XN), tp // 2, lax.rem(tp, 2)
    n = ZN * XN
    m = YN * 2
    half = YN // 2
    per = XN // 2
    picked, x, acc, act, p, q, pieces = (v[i] for i in ("picked", "x", "acc", "act", "p", "q", "pieces"))
    slots = picked.shape[1]
    count = ZN * per
    group = count * slots
    lanes = picked.shape[2]
    rows = v["columns"].shape[0]
    own = rows // m
    partner = {"tp": tp + 1 - 2 * c}

    def rows_of(i):
        return pl.ds(pl.multiple_of(i * own, own), own)

    def cols_of(i):
        return pl.ds(pl.multiple_of(i * lanes, lanes), lanes)

    barrier = pltpu.get_barrier_semaphore()
    greeted = 0
    for k in range(1, m):
        pl.semaphore_signal(barrier, inc=1, device_id={"tp": lax.rem(tp + k, m)}, device_id_type=MESH)
        greeted += 1
    for dz in range(ZN):
        for dx in range(XN):
            for core in range(2):
                if dz or dx:
                    peer = {"sp": sp_at(z, xx, dz, dx), "tp": y * 2 + core}
                    pl.semaphore_signal(barrier, inc=1, device_id=peer, device_id_type=MESH)
                    greeted += 1

    fetch = {}
    order = (
        "ka", "kb", "da", "db", "va", "vb", "qa", "qb", "ga", "gb", "head_gain", "routes", "affinity", "stream",
        "gain_mix", "gain_moe",
    )
    for i, name in enumerate(order):
        src = hbm[name].at[rows_of(tp), :] if name == "stream" else hbm[name]
        fetch[name] = pltpu.make_async_copy(src, v[name], v["early"].at[i])
        fetch[name].start()
    for i, name in enumerate(("pa", "pb")):
        fetch[name] = pltpu.make_async_copy(hbm[name], v["pj"].at[0, i], v["early"].at[len(order) + i])
        fetch[name].start()
    pairs = [(hbm[name].at[0], v[name]) for name in ("wg", "wu", "wd")]
    loads = [pltpu.make_async_copy(src, dst.at[0], v["loads"].at[i]) for i, (src, dst) in enumerate(pairs)]
    for load in loads:
        load.start()
    swaps = [
        remote(src, dst, v["swap_s"].at[i], v["swap_r"].at[i], partner)
        for i, (src, dst) in enumerate(
            [(hbm["pa"], v["pj"].at[1, 0]), (hbm["pb"], v["pj"].at[1, 1])] + [(s, d.at[1]) for s, d in pairs]
        )
    ]

    for name in ("ka", "kb", "da", "db", "va", "vb"):
        fetch[name].wait()
    cum, stack = v["cum"], v["stack"]
    keys_a = v["ka"][...].astype(F32).T
    keys_b = v["kb"][...].astype(F32)
    local_states(keys_a, v["va"][...], [v["da"][i].T for i in range(2)], 0, stack, cum)
    local_states(keys_b, v["vb"][...], [v["db"][i] for i in range(2)], DK_A, stack, cum)

    pl.semaphore_wait(barrier, greeted)

    xbox, agg, zbox, outx, states = (v[i] for i in ("xbox", "agg", "zbox", "outx", "states"))
    piece = outx.shape[2]

    def along_x(j):
        peer = lax.rem(xx + j, XN)
        return remote(stack.at[peer], xbox.at[xx], v["xs"].at[j], v["xr"].at[j], {"sp": z * XN + peer})

    def along_z(j):
        peer = lax.rem(z + j, ZN)
        way = jnp.where(peer > z, 0, 1)
        return remote(agg.at[way], zbox.at[z], v["zs"].at[j], v["zr"].at[j], {"sp": peer * XN + xx})

    def back_x(j):
        peer = lax.rem(xx + j, XN)
        return remote(outx.at[peer], states.at[xx], v["es"].at[j], v["er"].at[j], {"sp": z * XN + peer})

    far_x = sorted(range(1, XN), key=lambda j: -near(j, XN))
    far_z = sorted(range(1, ZN), key=lambda j: -near(j, ZN))
    for j in far_x:
        along_x(j).start()
    for swap in swaps:
        swap.start()
    xbox[xx] = stack[xx]
    zbox[z] = jnp.zeros_like(zbox[z])

    for name in ("qa", "qb"):
        fetch[name].wait()
    mixed, reach = v["mixed"], v["reach"]
    dv = v["va"].shape[1]
    local_mix(v["qa"][...].astype(F32).T, keys_a, v["va"][...], 0, cum, reach, 0, mixed)

    def load(block):
        block = block.astype(F32)
        return block[0:piece], block[piece : piece + 1] + block[piece + 1 : piece + 2]

    for j in range(1, XN):
        source = lax.rem(xx + XN - j, XN)
        remote(stack.at[source], xbox.at[source], v["xs"].at[j], v["xr"].at[j], {"sp": z * XN + source}).wait_recv()
    for way in range(2):
        state, fade = None, None
        for i in range(XN) if way == 0 else reversed(range(XN)):
            own_state, own_fade = load(xbox[i, way])
            state = own_state if state is None else jnp.exp(own_fade) * state + own_state
            fade = own_fade if fade is None else fade + own_fade
        agg[way, 0:piece] = state.astype(BF16)
        agg[way, piece : piece + FADES] = fade_rows(fade)
    for j in far_z:
        along_z(j).start()

    local_mix(v["qb"][...].astype(F32), keys_b, v["vb"][...], DK_A, cum, reach, dv, mixed)
    for name in ("routes", "affinity"):
        fetch[name].wait()
    routes, affinity = v["routes"][...], v["affinity"][...]
    lane = lax.broadcasted_iota(jnp.int32, (n, rows), 0)
    hots = [routes[i : i + 1] == lane for i in range(2)]
    named = sum(jnp.where(h, 1.0, 0.0) for h in hots)
    ii = lax.broadcasted_iota(jnp.int32, (rows, rows), 0)
    jj = lax.broadcasted_iota(jnp.int32, (rows, rows), 1)
    before = mm(named.astype(BF16), jnp.where(ii < jj, 1.0, 0.0).astype(BF16))
    place = [
        routes[i : i + 1] * slots
        + jnp.sum(jnp.where(hots[i], before, 0.0), axis=0, keepdims=True).astype(jnp.int32)
        for i in range(2)
    ]
    seat = lax.broadcasted_iota(jnp.int32, (n * slots, rows), 0)
    v["hot"][...] = jnp.where((seat == place[0]) | (seat == place[1]), 1.0, 0.0).astype(BF16)
    weights = [affinity[i : i + 1] / (affinity[0:1] + affinity[1:2]) for i in range(2)]
    mix = jnp.where(seat == place[0], weights[0], jnp.where(seat == place[1], weights[1], 0.0)).T
    high = mix.astype(BF16)
    v["mixhi"][...] = high
    v["mixlo"][...] = (mix - high.astype(F32)).astype(BF16)

    for j in range(1, ZN):
        source = lax.rem(z + ZN - j, ZN)
        remote(agg.at[0], zbox.at[source], v["zs"].at[j], v["zr"].at[j], {"sp": source * XN + xx}).wait_recv()
    keys = zbox.shape[2]
    ahead = jnp.zeros((piece, keys), F32)
    behind = jnp.zeros((piece, keys), F32)
    for i in range(ZN):
        state, fade = load(zbox[i])
        ahead = jnp.where(i < z, jnp.exp(fade) * ahead + state, ahead)
    for i in reversed(range(ZN)):
        state, fade = load(zbox[i])
        behind = jnp.where(i > z, jnp.exp(fade) * behind + state, behind)
    for i in range(XN):
        outx[i, 0] = ahead.astype(BF16)
        if i < XN - 1:
            state, fade = load(xbox[i, 0])
            ahead = jnp.exp(fade) * ahead + state
    for i in reversed(range(XN)):
        outx[i, 1] = behind.astype(BF16)
        if i > 0:
            state, fade = load(xbox[i, 1])
            behind = jnp.exp(fade) * behind + state
    for j in far_x:
        back_x(j).start()
    states[xx] = outx[xx]
    for name in ("ga", "gb", "head_gain", "pa", "pb", "stream", "gain_mix", "gain_moe"):
        fetch[name].wait()
    for j in range(1, XN):
        source = lax.rem(xx + XN - j, XN)
        remote(outx.at[source], states.at[source], v["es"].at[j], v["er"].at[j], {"sp": z * XN + source}).wait_recv()

    heads, hbox = v["heads"], v["hbox"]
    for i, (base, dk, gate) in enumerate(((0, DK_A, v["ga"]), (DK_A, DK_B, v["gb"]))):
        at = slice(base, base + dk)
        whole = mixed[:, i * dv : (i + 1) * dv]
        for way in range(2):
            start = states[:, way].reshape(dv, keys)
            whole = whole + mm_nt(reach[way, :, at], start[:, at])
        scale = lax.rsqrt(jnp.mean(whole * whole, axis=-1, keepdims=True) + 1e-06)
        value = (whole * scale * v["head_gain"][...] * silu(gate[...].astype(F32))).astype(BF16)
        value = value.reshape(YN, 2, own, dv)
        for core in range(2):
            heads[core, :, i * dv : (i + 1) * dv] = value[:, core].reshape(YN * own, dv)
    hand = remote(heads.at[1 - c], hbox, v["hs"].at[0], v["hs"].at[1], partner)
    hand.start()
    pj, pp = v["pj"], v["pp"]
    pp[...] = (mm(heads[c], pj[0].reshape(2 * dv, pj.shape[3]))).reshape(pp.shape)
    swaps[0].wait_recv()
    swaps[1].wait_recv()
    hand.wait_recv()
    pp[...] = pp[...] + (mm(hbox[...], pj[1].reshape(2 * dv, pj.shape[3]))).reshape(pp.shape)

    settled, moe_in, columns = v["settled"], v["moe_in"], v["columns"]
    cut = v["s1"].shape[4]

    def attn_part(o, k):
        return pp[lax.rem(y + o, YN), :, k * cut : (k + 1) * cut]

    def attn_done(k, total):
        settled[:, k * cut : (k + 1) * cut] = total

    sent_attn = ring_sum(
        y, c, CUTS, attn_part, lambda o: None, v["s1"], v["r1"], v["s1s"], v["s1r"], attn_done
    )
    value = layer_norm(v["stream"][...].astype(F32) + settled[...], v["gain_mix"][...])
    settled[...] = value
    moe_in[...] = value.astype(BF16)

    far_tp = sorted(range(1, m), key=lambda k: -near(k // 2, YN))

    def to_columns(k):
        peer = lax.rem(tp + k, m)
        return remote(moe_in.at[:, cols_of(peer)], columns.at[rows_of(tp), :], v["cs"].at[k], v["cr"].at[k], {"tp": peer})

    for k in far_tp:
        to_columns(k).start()
    columns[rows_of(tp), :] = moe_in[:, cols_of(tp)]
    for k in range(1, m):
        source = lax.rem(tp + m - k, m)
        remote(
            moe_in.at[:, cols_of(source)], columns.at[rows_of(source), :], v["cs"].at[k], v["cr"].at[k], {"tp": source}
        ).wait_recv()
    picked[...] = mm(v["hot"][...], columns[...]).astype(BF16).reshape(picked.shape)

    def dispatch(dz, dx):
        e = sp_at(z, xx, dz, dx)
        rz, rx = (-dz) % ZN, (-dx) % XN
        j = rz * per + rx // 2
        return remote(
            picked.at[e], x.at[y, c, j], v["ds"].at[dz * XN + dx], v["dr"].at[c, j], {"sp": e, "tp": y * 2 + dx % 2}
        )

    home = pltpu.make_async_copy(picked.at[sp], x.at[y, 0, 0], v["dr"].at[0, 0])
    offsets = sorted(
        [(dz, dx) for dz in range(ZN) for dx in range(XN)],
        key=lambda o: -(near(o[0], ZN) + near(o[1], XN)),
    )
    for dz, dx in offsets:
        if dz or dx:
            dispatch(dz, dx).start()
    pl.when(c == 0)(lambda: home.start())
    pl.when(c == 1)(lambda: dispatch(0, 0).start())

    def arrive(k, j):
        remote(picked.at[0], x.at[y, k, j], v["ds"].at[0], v["dr"].at[k, j], partner).wait_recv()

    def hop(way, h, k, behind=0):
        step = step_of(way)
        b = lax.rem(y + (h - 1 + behind) * (YN - step), YN)
        return remote(
            x.at[b, k], x.at[b, k], v["gs"].at[way, h - 1, k], v["gr"].at[way, h - 1, k],
            {"tp": lax.rem(y + step, YN) * 2 + c},
        )

    wg, wu, wd = v["wg"], v["wu"], v["wd"]

    def widen(b, first=False):
        at = pl.ds(pl.multiple_of(b * 2 * lanes, 2 * lanes), 2 * lanes)
        block = jnp.concatenate([x[b, k].reshape(group, lanes) for k in range(2)], axis=1)
        w = jnp.concatenate([ref[i, at, :] for ref in (wg, wu) for i in range(2)], axis=1)
        value = mm(block, w)
        acc[...] = value if first else acc[...] + value

    for k in range(2):
        for j in range(count):
            if k == 0 and j == 0:
                pl.when(c == 0)(lambda: home.wait())
                pl.when(c == 1)(lambda: arrive(0, 0))
            else:
                arrive(k, j)
        for way in range(2):
            if carried(way, 1, k, 2):
                hop(way, 1, k).start()
    for load_w in loads:
        load_w.wait()
    for swap in swaps[2:]:
        swap.wait_recv()
    widen(y, first=True)
    for h in range(1, half + 1):
        for k in range(2):
            for way in range(2):
                if carried(way, h, k, 2):
                    hop(way, h, k, 1).wait_recv()
                    if h < half and carried(way, h + 1, k, 2):
                        hop(way, h + 1, k).start()
        widen(lax.rem(y + YN - h, YN))
        if h < half:
            widen(lax.rem(y + h, YN))

    hidden = 2 * lanes
    act[...] = (silu(acc[:, :hidden]) * acc[:, hidden:]).astype(BF16)

    def narrow(o):
        b = lax.rem(y + o, YN)
        at = pl.ds(pl.multiple_of(b * hidden, hidden), hidden)
        p[o] = mm(act[...], jnp.concatenate([wd[i, :, at] for i in range(2)], axis=0))

    def give(k, j):
        rz = j // per
        rx = 2 * (j % per) + c
        o = ((-rz) % ZN) * XN + lax.rem(XN - rx, XN)
        return remote(
            q.at[k, j], pieces.at[sp], v["bs"].at[k, j], v["br"].at[o], {"sp": sp_at(z, xx, rz, rx), "tp": y * 2 + k}
        )

    back = pltpu.make_async_copy(q.at[0, 0], pieces.at[sp], v["br"].at[0])
    far_j = sorted(range(count), key=lambda j: -near(j // per, ZN))

    def moe_done(k, total):
        q[k] = total.astype(BF16).reshape(count, slots, lanes)
        for j in far_j:
            if k == 0 and j == 0:
                pl.when(c == 0)(lambda: back.start())
                pl.when(c == 1)(lambda: give(0, 0).start())
            else:
                give(k, j).start()

    sent_moe = ring_sum(
        y, c, 2, lambda o, k: p[o, :, k * lanes : (k + 1) * lanes], narrow, v["s2"], v["r2"], v["s2s"], v["s2r"],
        moe_done,
    )
    for dz in range(ZN):
        for dx in range(XN):
            o = dz * XN + dx
            e = sp_at(z, xx, dz, dx)
            coming = remote(q.at[0, 0], pieces.at[e], v["bs"].at[0, 0], v["br"].at[o], partner)
            if o == 0:
                pl.when(c == 0)(lambda: back.wait())
                pl.when(c == 1)(lambda: coming.wait_recv())
            else:
                coming.wait_recv()

    term, mixture = v["term"], v["mixture"]
    flat = pieces[...].reshape(n * slots, lanes)
    term[...] = (mm(v["mixhi"][...], flat) + mm(v["mixlo"][...], flat)).astype(BF16)

    def spread_rows(k):
        peer = lax.rem(tp + k, m)
        return remote(term.at[rows_of(peer), :], mixture.at[:, cols_of(tp)], v["fs"].at[k], v["fr"].at[k], {"tp": peer})

    for k in far_tp:
        spread_rows(k).start()
    mixture[:, cols_of(tp)] = term[rows_of(tp), :]
    for k in range(1, m):
        source = lax.rem(tp + m - k, m)
        remote(
            term.at[rows_of(source), :], mixture.at[:, cols_of(source)], v["fs"].at[k], v["fr"].at[k], {"tp": source}
        ).wait_recv()
    out[...] = layer_norm(settled[...] + mixture[...].astype(F32), v["gain_moe"][...]).astype(BF16)

    for j in range(1, XN):
        along_x(j).wait_send()
        back_x(j).wait_send()
    for j in range(1, ZN):
        along_z(j).wait_send()
    hand.wait_send()
    for swap in swaps:
        swap.wait_send()
    sent_attn()
    for k in range(1, m):
        to_columns(k).wait_send()
        spread_rows(k).wait_send()
    for dz, dx in offsets:
        if dz or dx:
            dispatch(dz, dx).wait_send()
    pl.when(c == 1)(lambda: dispatch(0, 0).wait_send())
    for way in range(2):
        for h in range(1, half + 1):
            for k in range(2):
                if carried(way, h, k, 2):
                    hop(way, h, k).wait_send()
    sent_moe()
    for k in range(2):
        for j in range(count):
            if k == 0 and j == 0:
                pl.when(c == 1)(lambda: give(0, 0).wait_send())
            else:
                give(k, j).wait_send()


def body(
    query_one, key_one, value_one, gate_one, decay_one, query_two, key_two, value_two, gate_two, decay_two,
    head_gain, proj_one, proj_two, stream, gain_mix, gain_moe, routes, affinity, expert_gate, expert_up,
    expert_down,
):
    rows, width = stream.shape
    dv = head_gain.shape[0]
    scratch = shapes_of(rows, dv, width)
    return pl.pallas_call(
        functools.partial(layer_kernel, tuple(scratch)),
        out_shape=jax.ShapeDtypeStruct((rows // (YN * 2), width), BF16),
        in_specs=[ANY] * len(INPUTS),
        out_specs=VMEM,
        scratch_shapes=list(scratch.values()),
        compiler_params=pltpu.CompilerParams(
            vmem_limit_bytes=56 * 2**20, collective_id=1, has_side_effects=True
        ),
    )(
        query_one.T, key_one.T, value_one, gate_one, jnp.swapaxes(decay_one, 1, 2), query_two, key_two, value_two,
        gate_two, decay_two, head_gain.reshape(1, -1), proj_one, proj_two, stream, gain_mix.reshape(1, -1),
        gain_moe.reshape(1, -1), routes.T, affinity.T, expert_gate, expert_up, expert_down,
    )


def solution(mesh):
    return jax.shard_map(
        body,
        mesh=mesh,
        in_specs=(
            P("sp", "tp"),
            P("sp", "tp"),
            P("sp", "tp"),
            P("sp", "tp"),
            P(None, "sp", "tp"),
            P("sp", "tp"),
            P("sp", "tp"),
            P("sp", "tp"),
            P("sp", "tp"),
            P(None, "sp", "tp"),
            P(),
            P("tp", None),
            P("tp", None),
            P("sp", None),
            P(),
            P(),
            P("sp", None),
            P("sp", None),
            P("sp", None, "tp"),
            P("sp", None, "tp"),
            P("sp", "tp", None),
        ),
        out_specs=P(("sp", "tp"), None),
        check_vma=False,
    )
```

time: 140 us -> 113 us (0.81)
  Pallas kernels: 136 us -> 112 us
  local copies, waits for them, and re-layouts: 4.28 us -> 1.47 us
    pallas_call x5 -> x1, Pallas kernels: 136 us -> 112 us  [body(): pl.pallas_call(functools.partial(layer_kernel, tuple(scratch)), out_shape...]
    unnamed x42 -> x1, local copies, waits for them, and re-layouts: 4.28 us -> 1.47 us
where the time goes in v2:
time: 113 us
  Pallas kernels  112 us (99%)
  local copies, waits for them, and re-layouts  1.47 us (1%)
    pallas_call x1, Pallas kernels, body(): pl.pallas_call(functools.partial(layer_kernel, tuple(scratch)), out_shape...  112 us

profile of v2, /device:TPU:1, one launch (start us, length us, event | category | flops | bytes accessed | tf_op | source)
XLA Modules:
  0.0 113.1 jit_solution(1376407280928139852)
XLA Ops:
  0.0 111.7 %shard_map.199 = bf16[16,2048]{1,0:T(8,128)(2,1)} custom-call(bf16[64,256]{1,0:T(8,128)(2,1)} %bitcast.9, bf16[64,256]{1,0:T(8,128)(2,1)} %bitcast.10, bf16[256,128]{1,0:T(8,128)(2,1)} %refs_2_.1, bf16[256,128]{1,0:T(8,128)(2,1)} %refs_3_.1, f32[2,64,256]{2,1,0:T(8,128)} %bitcast.8, bf16[256,128]{1,0:T(8,128)(2,1)} %refs_5_.1, bf16[256,128]{1,0:T(8,128)(2,1)} %refs_6_.1, ...), custom_call_target="tpu_custom_call" | custom-call | tf_op jit(solution)/shard_map/pallas_call | solution.py:653
  111.7 1.5 %copy.23 = bf16[16,2048]{1,0:T(8,128)(2,1)} copy(bf16[16,2048]{1,0:T(8,128)(2,1)} %shard_map.199) | data formatting | bytes 131072

commit v3 on v2

--- a/solution.py
+++ b/solution.py
@@ -13,6 +13,7 @@
 SHARPNESS = 16.0
 ZN, XN, YN = 8, 4, 8
 CUTS = 4
+GROUPS = 4
 FADES = 8
 F32 = jnp.float32
 BF16 = jnp.bfloat16
@@ -60,10 +61,6 @@
 
 def near(d, n):
     return min(d, n - d)
-
-
-def carried(way, d, k, cuts):
-    return d < YN // 2 or k // (cuts // 2) == way
 
 
 def step_of(way):
@@ -154,59 +151,58 @@
         mixed[at, column : column + dv] = inner[b]
 
 
-def ring_sum(y, c, cuts, part, prepare, s, r, ss, sr, finish):
+def ring_sum(y, c, order, jump, part, prepare, extra, s, r, ss, sr, finish):
     half = YN // 2
+    started = []
+
+    def mine(way, k):
+        return k // (len(order) // 2) == way
 
     def pass_sum(way, d, k):
+        step = jump if d == half else 1
         return remote(
             s.at[way, d - 1, k], r.at[way, d - 1, k], ss.at[way, d - 1, k], sr.at[way, d - 1, k],
-            {"tp": lax.rem(y + step_of(way), YN) * 2 + c},
+            {"tp": lax.rem(y + (step if way == 0 else YN - step), YN) * 2 + c},
         )
 
-    def order(way):
-        mine = [k for k in range(cuts) if k // (cuts // 2) == way]
-        return mine, [k for k in range(cuts) if k not in mine]
-
-    def send(way, d, k):
-        total = part(d if way == 0 else YN - d, k)
-        if d < half and carried(way, d + 1, k, cuts):
+    def collect(total, way, d, k):
+        if d + 1 < half:
             pass_sum(way, d + 1, k).wait_recv()
             total = total + r[way, d, k].astype(F32)
-        s[way, d - 1, k] = total.astype(BF16)
-        pass_sum(way, d, k).start()
-
-    prepare(half)
-    for turn in range(cuts // 2):
-        for way in range(2):
-            send(way, half, order(way)[0][turn])
+        if jump and mine(way, k) and half - jump == d:
+            pass_sum(way, half, k).wait_recv()
+            total = total + r[way, half - 1, k].astype(F32)
+        return total
+
+    def send(way, d, k):
+        s[way, d - 1, k] = collect(part(d if way == 0 else YN - d, k), way, d, k).astype(BF16)
+        copy = pass_sum(way, d, k)
+        copy.start()
+        started.append(copy)
+
+    if jump:
+        prepare(half)
+        for k in order:
+            for way in range(2):
+                if mine(way, k):
+                    send(way, half, k)
     for d in range(half - 1, 0, -1):
         prepare(d)
         prepare(YN - d)
-        for turn in range(cuts):
+        for k in order:
             for way in range(2):
-                near_first, late = order(way)
-                ks = late + near_first if d == half - 1 else near_first + late
-                if d < half - 1 and half > 2:
-                    ks = late + near_first
-                send(way, d, ks[turn])
+                send(way, d, k)
+        if d == half - 1:
+            extra()
+    if half == 1:
+        extra()
     prepare(0)
-    for turn in range(cuts):
-        k = (cuts // 2 * (turn % 2) + turn // 2) % cuts
+    for k in order:
         total = part(0, k)
         for way in range(2):
-            if carried(way, 1, k, cuts):
-                pass_sum(way, 1, k).wait_recv()
-                total = total + r[way, 0, k].astype(F32)
+            total = collect(total, way, 0, k)
         finish(k, total)
-
-    def settle_sends():
-        for way in range(2):
-            for d in range(1, half + 1):
-                for k in range(cuts):
-                    if carried(way, d, k, cuts):
-                        pass_sum(way, d, k).wait_send()
-
-    return settle_sends
+    return started
 
 
 INPUTS = (
@@ -228,6 +224,8 @@
     piece = dv // XN
     big = piece + FADES
     mine = rows // 2
+    groups = min(GROUPS, count)
+    hops = max(1, half - 1)
     cut = width // CUTS
     v = pltpu.VMEM
     return dict(
@@ -246,15 +244,17 @@
         hbox=v((mine, 2 * dv), BF16), hs=DMA((2,)), pp=v((YN, own, width), F32),
         s1=v((2, half, CUTS, own, cut), BF16), r1=v((2, half, CUTS, own, cut), BF16),
         s1s=DMA((2, half, CUTS)), s1r=DMA((2, half, CUTS)), settled=v((own, width), F32),
-        moe_in=v((own, width), BF16), columns=v((rows, lanes), BF16), cs=DMA((m,)), cr=DMA((m,)),
+        moe_in=v((2, YN, own, lanes), BF16), columns=v((2, rows, lanes), BF16), cs=DMA((m,)), cr=DMA((m,)),
         hot=v((n * slots, rows), BF16),
-        mixhi=v((rows, n * slots), BF16), mixlo=v((rows, n * slots), BF16), picked=v((n, slots, lanes), BF16),
-        x=v((YN, 2, count, slots, lanes), BF16), acc=v((group, 4 * lanes), F32), act=v((group, 2 * lanes), BF16),
-        p=v((YN, group, 2 * lanes), F32), s2=v((2, half, 2, group, lanes), BF16),
-        r2=v((2, half, 2, group, lanes), BF16), s2s=DMA((2, half, 2)), s2r=DMA((2, half, 2)),
-        q=v((2, count, slots, lanes), BF16), pieces=v((n, slots, lanes), BF16), term=v((rows, lanes), BF16),
-        mixture=v((own, width), BF16), ds=DMA((n,)), dr=DMA((2, count)), gs=DMA((2, half, 2)), gr=DMA((2, half, 2)),
-        bs=DMA((2, count)), br=DMA((n,)), fs=DMA((m,)), fr=DMA((m,)),
+        mixhi=v((rows, n * slots), BF16), mixlo=v((rows, n * slots), BF16), picked=v((2, n, slots, lanes), BF16),
+        x=v((YN, groups, 2, count // groups, slots, lanes), BF16), acc=v((group, 4 * lanes), F32),
+        act=v((group, 2 * lanes), BF16), p=v((YN, group, 2 * lanes), F32),
+        s2=v((2, hops, groups, group // groups, 2 * lanes), BF16),
+        r2=v((2, hops, groups, group // groups, 2 * lanes), BF16), s2s=DMA((2, hops, groups)),
+        s2r=DMA((2, hops, groups)), q=v((2, 2, count, slots, lanes), BF16), pieces=v((2, n, slots, lanes), BF16),
+        term=v((2, rows, lanes), BF16), mixbox=v((m, 2, own, lanes), BF16), ds=DMA((2, n)), dr=DMA((2, 2, count)),
+        gs=DMA((2, hops, groups)), gr=DMA((2, hops, groups)), bs=DMA((2, 2, count)), br=DMA((2, n)),
+        fs=DMA((m,)), fr=DMA((m,)),
     )
 
 
@@ -270,19 +270,18 @@
     half = YN // 2
     per = XN // 2
     picked, x, acc, act, p, q, pieces = (v[i] for i in ("picked", "x", "acc", "act", "p", "q", "pieces"))
-    slots = picked.shape[1]
+    slots = picked.shape[2]
     count = ZN * per
     group = count * slots
-    lanes = picked.shape[2]
-    rows = v["columns"].shape[0]
+    lanes = picked.shape[3]
+    groups = x.shape[1]
+    size = count // groups
+    rows = v["columns"].shape[1]
     own = rows // m
     partner = {"tp": tp + 1 - 2 * c}
 
     def rows_of(i):
         return pl.ds(pl.multiple_of(i * own, own), own)
-
-    def cols_of(i):
-        return pl.ds(pl.multiple_of(i * lanes, lanes), lanes)
 
     barrier = pltpu.get_barrier_semaphore()
     greeted = 0
@@ -463,56 +462,87 @@
     def attn_done(k, total):
         settled[:, k * cut : (k + 1) * cut] = total
 
-    sent_attn = ring_sum(
-        y, c, CUTS, attn_part, lambda o: None, v["s1"], v["r1"], v["s1s"], v["s1r"], attn_done
+    sent = ring_sum(
+        y, c, [k // 2 + CUTS // 2 * (k % 2) for k in range(CUTS)], min(2, half), attn_part, lambda o: None,
+        lambda: None, v["s1"], v["r1"], v["s1s"], v["s1r"], attn_done,
     )
     value = layer_norm(v["stream"][...].astype(F32) + settled[...], v["gain_mix"][...])
     settled[...] = value
-    moe_in[...] = value.astype(BF16)
+    value = value.astype(BF16)
+    for i in range(m):
+        moe_in[i // YN, i % YN] = value[:, i * lanes : (i + 1) * lanes]
 
     far_tp = sorted(range(1, m), key=lambda k: -near(k // 2, YN))
 
     def to_columns(k):
         peer = lax.rem(tp + k, m)
-        return remote(moe_in.at[:, cols_of(peer)], columns.at[rows_of(tp), :], v["cs"].at[k], v["cr"].at[k], {"tp": peer})
+        return remote(
+            moe_in.at[:, lax.rem(peer, YN)], columns.at[:, rows_of(tp), :], v["cs"].at[k], v["cr"].at[k], {"tp": peer}
+        )
 
     for k in far_tp:
         to_columns(k).start()
-    columns[rows_of(tp), :] = moe_in[:, cols_of(tp)]
+    columns[:, rows_of(tp), :] = moe_in[:, lax.rem(tp, YN)]
     for k in range(1, m):
         source = lax.rem(tp + m - k, m)
         remote(
-            moe_in.at[:, cols_of(source)], columns.at[rows_of(source), :], v["cs"].at[k], v["cr"].at[k], {"tp": source}
+            moe_in.at[:, 0], columns.at[:, rows_of(source), :], v["cs"].at[k], v["cr"].at[k], {"tp": source}
         ).wait_recv()
-    picked[...] = mm(v["hot"][...], columns[...]).astype(BF16).reshape(picked.shape)
-
-    def dispatch(dz, dx):
+    wide = mm(v["hot"][...], jnp.concatenate([columns[0], columns[1]], axis=1)).astype(BF16)
+    for i in range(2):
+        picked[i] = wide[:, i * lanes : (i + 1) * lanes].reshape(n, slots, lanes)
+
+    z_order = sorted(range(ZN), key=lambda d: near(d, ZN))
+    z_rank = [z_order.index(d) for d in range(ZN)]
+
+    def block_of(o):
+        return lax.rem(y + o * half, YN)
+
+    def seat_of(b, k, j):
+        return x.at[b, j // size, k, j % size]
+
+    def dispatch(o, dz, dx):
         e = sp_at(z, xx, dz, dx)
         rz, rx = (-dz) % ZN, (-dx) % XN
-        j = rz * per + rx // 2
+        j = z_rank[rz] * per + rx // 2
+        b = block_of(o)
         return remote(
-            picked.at[e], x.at[y, c, j], v["ds"].at[dz * XN + dx], v["dr"].at[c, j], {"sp": e, "tp": y * 2 + dx % 2}
+            picked.at[b // half, e], seat_of(b, c, j), v["ds"].at[o, dz * XN + dx], v["dr"].at[o, c, j],
+            {"sp": e, "tp": y * 2 + dx % 2},
         )
 
-    home = pltpu.make_async_copy(picked.at[sp], x.at[y, 0, 0], v["dr"].at[0, 0])
+    homes = [
+        pltpu.make_async_copy(picked.at[block_of(o) // half, sp], seat_of(block_of(o), 0, 0), v["dr"].at[o, 0, 0])
+        for o in range(2)
+    ]
     offsets = sorted(
-        [(dz, dx) for dz in range(ZN) for dx in range(XN)],
-        key=lambda o: -(near(o[0], ZN) + near(o[1], XN)),
-    )
-    for dz, dx in offsets:
-        if dz or dx:
-            dispatch(dz, dx).start()
-    pl.when(c == 0)(lambda: home.start())
-    pl.when(c == 1)(lambda: dispatch(0, 0).start())
-
-    def arrive(k, j):
-        remote(picked.at[0], x.at[y, k, j], v["ds"].at[0], v["dr"].at[k, j], partner).wait_recv()
-
-    def hop(way, h, k, behind=0):
+        [(dz, dx) for dz in range(ZN) for dx in range(XN)], key=lambda o: near(o[0], ZN) + near(o[1], XN)
+    )
+    def send_wave(o):
+        for dz, dx in offsets:
+            if dz or dx:
+                dispatch(o, dz, dx).start()
+        pl.when(c == 0)(lambda: homes[o].start())
+        pl.when(c == 1)(lambda: dispatch(o, 0, 0).start())
+
+    send_wave(0)
+
+    def arrive(o, j):
+        for k in range(2):
+            coming = remote(
+                picked.at[0, 0], seat_of(block_of(o), k, j), v["ds"].at[0, 0], v["dr"].at[o, k, j], partner
+            )
+            if k == 0 and j == 0:
+                pl.when(c == 0)(lambda: homes[o].wait())
+                pl.when(c == 1)(lambda: coming.wait_recv())
+            else:
+                coming.wait_recv()
+
+    def hop(way, h, g, behind=0):
         step = step_of(way)
         b = lax.rem(y + (h - 1 + behind) * (YN - step), YN)
         return remote(
-            x.at[b, k], x.at[b, k], v["gs"].at[way, h - 1, k], v["gr"].at[way, h - 1, k],
+            x.at[b, g], x.at[b, g], v["gs"].at[way, h - 1, g], v["gr"].at[way, h - 1, g],
             {"tp": lax.rem(y + step, YN) * 2 + c},
         )
 
@@ -520,36 +550,39 @@
 
     def widen(b, first=False):
         at = pl.ds(pl.multiple_of(b * 2 * lanes, 2 * lanes), 2 * lanes)
-        block = jnp.concatenate([x[b, k].reshape(group, lanes) for k in range(2)], axis=1)
+        block = jnp.concatenate([x[b, :, k].reshape(group, lanes) for k in range(2)], axis=1)
         w = jnp.concatenate([ref[i, at, :] for ref in (wg, wu) for i in range(2)], axis=1)
         value = mm(block, w)
         acc[...] = value if first else acc[...] + value
 
-    for k in range(2):
-        for j in range(count):
-            if k == 0 and j == 0:
-                pl.when(c == 0)(lambda: home.wait())
-                pl.when(c == 1)(lambda: arrive(0, 0))
-            else:
-                arrive(k, j)
+    for g in range(groups):
+        for j in range(g * size, (g + 1) * size):
+            arrive(0, j)
         for way in range(2):
-            if carried(way, 1, k, 2):
-                hop(way, 1, k).start()
+            if half > 1:
+                hop(way, 1, g).start()
+    send_wave(1)
     for load_w in loads:
         load_w.wait()
     for swap in swaps[2:]:
         swap.wait_recv()
     widen(y, first=True)
-    for h in range(1, half + 1):
-        for k in range(2):
+    for h in range(1, half):
+        if h == half - 1:
+            for j in range(count):
+                arrive(1, j)
+            widen(block_of(1))
+        for g in range(groups):
             for way in range(2):
-                if carried(way, h, k, 2):
-                    hop(way, h, k, 1).wait_recv()
-                    if h < half and carried(way, h + 1, k, 2):
-                        hop(way, h + 1, k).start()
+                hop(way, h, g, 1).wait_recv()
+                if h < half - 1:
+                    hop(way, h + 1, g).start()
         widen(lax.rem(y + YN - h, YN))
-        if h < half:
-            widen(lax.rem(y + h, YN))
+        widen(lax.rem(y + h, YN))
+    if half == 1:
+        for j in range(count):
+            arrive(1, j)
+        widen(block_of(1))
 
     hidden = 2 * lanes
     act[...] = (silu(acc[:, :hidden]) * acc[:, hidden:]).astype(BF16)
@@ -559,58 +592,81 @@
         at = pl.ds(pl.multiple_of(b * hidden, hidden), hidden)
         p[o] = mm(act[...], jnp.concatenate([wd[i, :, at] for i in range(2)], axis=0))
 
-    def give(k, j):
-        rz = j // per
+    def give(o, k, j):
+        rz = z_order[j // per]
         rx = 2 * (j % per) + c
-        o = ((-rz) % ZN) * XN + lax.rem(XN - rx, XN)
+        back = ((-rz) % ZN) * XN + lax.rem(XN - rx, XN)
         return remote(
-            q.at[k, j], pieces.at[sp], v["bs"].at[k, j], v["br"].at[o], {"sp": sp_at(z, xx, rz, rx), "tp": y * 2 + k}
+            q.at[o, k, j], pieces.at[o, sp], v["bs"].at[o, k, j], v["br"].at[o, back],
+            {"sp": sp_at(z, xx, rz, rx), "tp": y * 2 + k},
         )
 
-    back = pltpu.make_async_copy(q.at[0, 0], pieces.at[sp], v["br"].at[0])
-    far_j = sorted(range(count), key=lambda j: -near(j // per, ZN))
-
-    def moe_done(k, total):
-        q[k] = total.astype(BF16).reshape(count, slots, lanes)
-        for j in far_j:
+    returns = [pltpu.make_async_copy(q.at[o, 0, 0], pieces.at[o, sp], v["br"].at[o, 0]) for o in range(2)]
+
+    def give_back(o, j):
+        for k in range(2):
             if k == 0 and j == 0:
-                pl.when(c == 0)(lambda: back.start())
-                pl.when(c == 1)(lambda: give(0, 0).start())
+                pl.when(c == 0)(lambda: returns[o].start())
+                pl.when(c == 1)(lambda: give(o, 0, 0).start())
             else:
-                give(k, j).start()
-
-    sent_moe = ring_sum(
-        y, c, 2, lambda o, k: p[o, :, k * lanes : (k + 1) * lanes], narrow, v["s2"], v["r2"], v["s2s"], v["s2r"],
-        moe_done,
-    )
-    for dz in range(ZN):
-        for dx in range(XN):
-            o = dz * XN + dx
-            e = sp_at(z, xx, dz, dx)
-            coming = remote(q.at[0, 0], pieces.at[e], v["bs"].at[0, 0], v["br"].at[o], partner)
-            if o == 0:
-                pl.when(c == 0)(lambda: back.wait())
-                pl.when(c == 1)(lambda: coming.wait_recv())
-            else:
-                coming.wait_recv()
-
-    term, mixture = v["term"], v["mixture"]
-    flat = pieces[...].reshape(n * slots, lanes)
-    term[...] = (mm(v["mixhi"][...], flat) + mm(v["mixlo"][...], flat)).astype(BF16)
+                give(o, k, j).start()
+
+    def opposite():
+        narrow(half)
+        for k in range(2):
+            q[1, k] = p[half, :, k * lanes : (k + 1) * lanes].astype(BF16).reshape(count, slots, lanes)
+        for j in reversed(range(count)):
+            give_back(1, j)
+
+    tall = group // groups
+
+    def moe_done(g, total):
+        total = total.astype(BF16)
+        js = range(g * size, (g + 1) * size)
+        for k in range(2):
+            q[0, k, g * size : (g + 1) * size] = total[:, k * lanes : (k + 1) * lanes].reshape(size, slots, lanes)
+        for j in reversed(js):
+            give_back(0, j)
+
+    sent += ring_sum(
+        y, c, list(reversed(range(groups))), 0, lambda o, g: p[o, g * tall : (g + 1) * tall, :], narrow, opposite,
+        v["s2"], v["r2"], v["s2s"], v["s2r"], moe_done,
+    )
+    for o in (1, 0):
+        for dz in range(ZN):
+            for dx in range(XN):
+                i = dz * XN + dx
+                coming = remote(
+                    q.at[0, 0, 0], pieces.at[o, sp_at(z, xx, dz, dx)], v["bs"].at[0, 0, 0], v["br"].at[o, i], partner
+                )
+                if i == 0:
+                    pl.when(c == 0)(lambda: returns[o].wait())
+                    pl.when(c == 1)(lambda: coming.wait_recv())
+                else:
+                    coming.wait_recv()
+
+    term, mixbox = v["term"], v["mixbox"]
+    flat = jnp.concatenate([pieces[o].reshape(n * slots, lanes) for o in range(2)], axis=1)
+    total = (mm(v["mixhi"][...], flat) + mm(v["mixlo"][...], flat)).astype(BF16)
+    for o in range(2):
+        term[o] = total[:, o * lanes : (o + 1) * lanes]
 
     def spread_rows(k):
         peer = lax.rem(tp + k, m)
-        return remote(term.at[rows_of(peer), :], mixture.at[:, cols_of(tp)], v["fs"].at[k], v["fr"].at[k], {"tp": peer})
+        return remote(term.at[:, rows_of(peer), :], mixbox.at[tp], v["fs"].at[k], v["fr"].at[k], {"tp": peer})
 
     for k in far_tp:
         spread_rows(k).start()
-    mixture[:, cols_of(tp)] = term[rows_of(tp), :]
+    mixbox[tp] = term[:, rows_of(tp), :]
     for k in range(1, m):
         source = lax.rem(tp + m - k, m)
         remote(
-            term.at[rows_of(source), :], mixture.at[:, cols_of(source)], v["fs"].at[k], v["fr"].at[k], {"tp": source}
+            term.at[:, rows_of(0), :], mixbox.at[source], v["fs"].at[k], v["fr"].at[k], {"tp": source}
         ).wait_recv()
-    out[...] = layer_norm(settled[...] + mixture[...].astype(F32), v["gain_moe"][...]).astype(BF16)
+    mixture = jnp.concatenate(
+        [mixbox[i, 0].astype(F32) + mixbox[(i + YN) % m, 1].astype(F32) for i in range(m)], axis=1
+    )
+    out[...] = layer_norm(settled[...] + mixture, v["gain_moe"][...]).astype(BF16)
 
     for j in range(1, XN):
         along_x(j).wait_send()
@@ -620,26 +676,26 @@
     hand.wait_send()
     for swap in swaps:
         swap.wait_send()
-    sent_attn()
+    for copy in sent:
+        copy.wait_send()
     for k in range(1, m):
         to_columns(k).wait_send()
         spread_rows(k).wait_send()
-    for dz, dx in offsets:
-        if dz or dx:
-            dispatch(dz, dx).wait_send()
-    pl.when(c == 1)(lambda: dispatch(0, 0).wait_send())
+    for o in range(2):
+        for dz, dx in offsets:
+            if dz or dx:
+                dispatch(o, dz, dx).wait_send()
+        pl.when(c == 1)(lambda: dispatch(o, 0, 0).wait_send())
+        for k in range(2):
+            for j in range(count):
+                if k == 0 and j == 0:
+                    pl.when(c == 1)(lambda: give(o, 0, 0).wait_send())
+                else:
+                    give(o, k, j).wait_send()
     for way in range(2):
-        for h in range(1, half + 1):
-            for k in range(2):
-                if carried(way, h, k, 2):
-                    hop(way, h, k).wait_send()
-    sent_moe()
-    for k in range(2):
-        for j in range(count):
-            if k == 0 and j == 0:
-                pl.when(c == 1)(lambda: give(0, 0).wait_send())
-            else:
-                give(k, j).wait_send()
+        for h in range(1, half):
+            for g in range(groups):
+                hop(way, h, g).wait_send()
 
 
 def body(

time: 113 us -> 105 us (0.929)
  Pallas kernels: 112 us -> 104 us
    pallas_call x1, Pallas kernels: 112 us -> 104 us  [body(): pl.pallas_call(functools.partial(layer_kernel, tuple(scratch)), out_shape...]
where the time goes in v3:
time: 105 us
  Pallas kernels  104 us (99%)
  local copies, waits for them, and re-layouts  1.47 us (1%)
    pallas_call x1, Pallas kernels, body(): pl.pallas_call(functools.partial(layer_kernel, tuple(scratch)), out_shape...  104 us

profile of v3, /device:TPU:1, one launch (start us, length us, event | category | flops | bytes accessed | tf_op | source)
XLA Modules:
  0.0 105.2 jit_solution(18203719092726394003)
XLA Ops:
  0.0 103.7 %shard_map.199 = bf16[16,2048]{1,0:T(8,128)(2,1)} custom-call(bf16[64,256]{1,0:T(8,128)(2,1)} %bitcast.9, bf16[64,256]{1,0:T(8,128)(2,1)} %bitcast.10, bf16[256,128]{1,0:T(8,128)(2,1)} %refs_2_.1, bf16[256,128]{1,0:T(8,128)(2,1)} %refs_3_.1, f32[2,64,256]{2,1,0:T(8,128)} %bitcast.8, bf16[256,128]{1,0:T(8,128)(2,1)} %refs_5_.1, bf16[256,128]{1,0:T(8,128)(2,1)} %refs_6_.1, ...), custom_call_target="tpu_custom_call" | custom-call | tf_op jit(solution)/shard_map/pallas_call | solution.py:709
  103.7 1.5 %copy.23 = bf16[16,2048]{1,0:T(8,128)(2,1)} copy(bf16[16,2048]{1,0:T(8,128)(2,1)} %shard_map.199) | data formatting | bytes 131072

commit v4 on v3

--- a/solution.py
+++ b/solution.py
@@ -13,7 +13,8 @@
 SHARPNESS = 16.0
 ZN, XN, YN = 8, 4, 8
 CUTS = 4
-GROUPS = 4
+GROUPS = 8
+LAG = 20
 FADES = 8
 F32 = jnp.float32
 BF16 = jnp.bfloat16
@@ -153,7 +154,6 @@
 
 def ring_sum(y, c, order, jump, part, prepare, extra, s, r, ss, sr, finish):
     half = YN // 2
-    started = []
 
     def mine(way, k):
         return k // (len(order) // 2) == way
@@ -161,24 +161,31 @@
     def pass_sum(way, d, k):
         step = jump if d == half else 1
         return remote(
-            s.at[way, d - 1, k], r.at[way, d - 1, k], ss.at[way, d - 1, k], sr.at[way, d - 1, k],
+            s.at[way, d - 1, k], r.at[way, d - 1, k], ss.at[int(d == half)], sr.at[d - 1, k],
             {"tp": lax.rem(y + (step if way == 0 else YN - step), YN) * 2 + c},
         )
 
+    def landed(d, k):
+        box = r.at[:, d - 1, k]
+        remote(box, box, ss.at[0], sr.at[d - 1, k], {"tp": y * 2 + 1 - c}).wait_recv()
+
     def collect(total, way, d, k):
         if d + 1 < half:
-            pass_sum(way, d + 1, k).wait_recv()
             total = total + r[way, d, k].astype(F32)
         if jump and mine(way, k) and half - jump == d:
-            pass_sum(way, half, k).wait_recv()
             total = total + r[way, half - 1, k].astype(F32)
         return total
 
+    def await_for(d, k):
+        if d + 1 < half:
+            landed(d + 1, k)
+        if jump and half - jump == d:
+            way = int(mine(1, k))
+            pass_sum(way, half, k).wait_recv()
+
     def send(way, d, k):
         s[way, d - 1, k] = collect(part(d if way == 0 else YN - d, k), way, d, k).astype(BF16)
-        copy = pass_sum(way, d, k)
-        copy.start()
-        started.append(copy)
+        pass_sum(way, d, k).start()
 
     if jump:
         prepare(half)
@@ -190,6 +197,7 @@
         prepare(d)
         prepare(YN - d)
         for k in order:
+            await_for(d, k)
             for way in range(2):
                 send(way, d, k)
         if d == half - 1:
@@ -199,10 +207,16 @@
     prepare(0)
     for k in order:
         total = part(0, k)
+        await_for(0, k)
         for way in range(2):
             total = collect(total, way, 0, k)
         finish(k, total)
-    return started
+    if half > 1:
+        whole = s.at[:, 0 : half - 1]
+        remote(whole, whole, ss.at[0], sr.at[0, 0], {"tp": y * 2 + 1 - c}).wait_send()
+    if jump:
+        whole = s.at[:, half - 1, 0 : len(order) // 2]
+        remote(whole, whole, ss.at[1], sr.at[0, 0], {"tp": y * 2 + 1 - c}).wait_send()
 
 
 INPUTS = (
@@ -235,26 +249,26 @@
         stream=v((own, width), BF16), gain_mix=v((1, width), F32), gain_moe=v((1, width), F32),
         routes=v((2, rows), jnp.int32), affinity=v((2, rows), F32),
         pj=v((2, 2, dv, width), BF16), wg=v((2, width, lanes), BF16), wu=v((2, width, lanes), BF16),
-        wd=v((2, lanes, width), BF16), early=DMA((19,)), loads=DMA((3,)), swap_s=DMA((5,)), swap_r=DMA((5,)),
+        wd=v((2, lanes, width), BF16), early=DMA((16,)), loads=DMA((3,)), swap_s=DMA((5,)), swap_r=DMA((5,)),
         cum=v((2, rows, keys), F32), stack=v((XN, 2, big, keys), BF16), xbox=v((XN, 2, big, keys), BF16),
         agg=v((2, big, keys), BF16), zbox=v((ZN, big, keys), BF16), outx=v((XN, 2, piece, keys), BF16),
-        states=v((XN, 2, piece, keys), BF16), xs=DMA((XN,)), xr=DMA((XN,)), zs=DMA((ZN,)), zr=DMA((ZN,)),
-        es=DMA((XN,)), er=DMA((XN,)),
+        states=v((XN, 2, piece, keys), BF16), xs=DMA, xr=DMA, zs=DMA, zr=DMA,
+        es=DMA, er=DMA,
         mixed=v((rows, 2 * dv), F32), reach=v((2, rows, keys), BF16), heads=v((2, mine, 2 * dv), BF16),
         hbox=v((mine, 2 * dv), BF16), hs=DMA((2,)), pp=v((YN, own, width), F32),
         s1=v((2, half, CUTS, own, cut), BF16), r1=v((2, half, CUTS, own, cut), BF16),
-        s1s=DMA((2, half, CUTS)), s1r=DMA((2, half, CUTS)), settled=v((own, width), F32),
-        moe_in=v((2, YN, own, lanes), BF16), columns=v((2, rows, lanes), BF16), cs=DMA((m,)), cr=DMA((m,)),
+        s1s=DMA((2,)), s1r=DMA((half, CUTS)), settled=v((own, width), F32),
+        moe_in=v((2, YN, own, lanes), BF16), columns=v((2, rows, lanes), BF16), cs=DMA, cr=DMA,
         hot=v((n * slots, rows), BF16),
         mixhi=v((rows, n * slots), BF16), mixlo=v((rows, n * slots), BF16), picked=v((2, n, slots, lanes), BF16),
         x=v((YN, groups, 2, count // groups, slots, lanes), BF16), acc=v((group, 4 * lanes), F32),
         act=v((group, 2 * lanes), BF16), p=v((YN, group, 2 * lanes), F32),
         s2=v((2, hops, groups, group // groups, 2 * lanes), BF16),
-        r2=v((2, hops, groups, group // groups, 2 * lanes), BF16), s2s=DMA((2, hops, groups)),
-        s2r=DMA((2, hops, groups)), q=v((2, 2, count, slots, lanes), BF16), pieces=v((2, n, slots, lanes), BF16),
-        term=v((2, rows, lanes), BF16), mixbox=v((m, 2, own, lanes), BF16), ds=DMA((2, n)), dr=DMA((2, 2, count)),
-        gs=DMA((2, hops, groups)), gr=DMA((2, hops, groups)), bs=DMA((2, 2, count)), br=DMA((2, n)),
-        fs=DMA((m,)), fr=DMA((m,)),
+        r2=v((2, hops, groups, group // groups, 2 * lanes), BF16), s2s=DMA((2,)),
+        s2r=DMA((hops, groups)), q=v((2, 2, count, slots, lanes), BF16), pieces=v((2, n, slots, lanes), BF16),
+        term=v((2, rows, lanes), BF16), mixbox=v((2, m, own, lanes), BF16), ds=DMA((2, 2)), dr=DMA((groups + 1,)),
+        gs=DMA, gr=DMA((hops, groups)), bs=DMA((2, 2)), br=DMA((2,)),
+        fs=DMA((2,)), fr=DMA((2,)),
     )
 
 
@@ -283,19 +297,6 @@
     def rows_of(i):
         return pl.ds(pl.multiple_of(i * own, own), own)
 
-    barrier = pltpu.get_barrier_semaphore()
-    greeted = 0
-    for k in range(1, m):
-        pl.semaphore_signal(barrier, inc=1, device_id={"tp": lax.rem(tp + k, m)}, device_id_type=MESH)
-        greeted += 1
-    for dz in range(ZN):
-        for dx in range(XN):
-            for core in range(2):
-                if dz or dx:
-                    peer = {"sp": sp_at(z, xx, dz, dx), "tp": y * 2 + core}
-                    pl.semaphore_signal(barrier, inc=1, device_id=peer, device_id_type=MESH)
-                    greeted += 1
-
     fetch = {}
     order = (
         "ka", "kb", "da", "db", "va", "vb", "qa", "qb", "ga", "gb", "head_gain", "routes", "affinity", "stream",
@@ -303,10 +304,26 @@
     )
     for i, name in enumerate(order):
         src = hbm[name].at[rows_of(tp), :] if name == "stream" else hbm[name]
-        fetch[name] = pltpu.make_async_copy(src, v[name], v["early"].at[i])
-        fetch[name].start()
+        fetch[name] = pltpu.make_async_copy(src, v[name], v["early"].at[max(0, i - 5)])
+        if i < 6:
+            fetch[name].start()
+    barrier = pltpu.get_barrier_semaphore()
+    def far(dz, dx, dy):
+        return near(dz, ZN) + near(dx, XN) + near(dy, YN)
+
+    friends = [
+        (far(dz, dx, 0), {"sp": sp_at(z, xx, dz, dx), "tp": y * 2 + core})
+        for dz in range(ZN) for dx in range(XN) for core in range(2) if dz or dx
+    ] + [(far(0, 0, k // 2), {"tp": lax.rem(tp + k, m)}) for k in range(1, m)]
+    for _, peer in sorted(friends, key=lambda f: -f[0]):
+        pl.semaphore_signal(barrier, inc=1, device_id=peer, device_id_type=MESH)
+    greeted = len(friends)
+
+    for i, name in enumerate(order):
+        if i >= 6:
+            fetch[name].start()
     for i, name in enumerate(("pa", "pb")):
-        fetch[name] = pltpu.make_async_copy(hbm[name], v["pj"].at[0, i], v["early"].at[len(order) + i])
+        fetch[name] = pltpu.make_async_copy(hbm[name], v["pj"].at[0, i], v["early"].at[len(order) - 5])
         fetch[name].start()
     pairs = [(hbm[name].at[0], v[name]) for name in ("wg", "wu", "wd")]
     loads = [pltpu.make_async_copy(src, dst.at[0], v["loads"].at[i]) for i, (src, dst) in enumerate(pairs)]
@@ -319,8 +336,8 @@
         )
     ]
 
-    for name in ("ka", "kb", "da", "db", "va", "vb"):
-        fetch[name].wait()
+    first = acc.at[0 : rows * 19 * DK_B // (16 * lanes)]
+    pltpu.make_async_copy(first, first, v["early"].at[0]).wait()
     cum, stack = v["cum"], v["stack"]
     keys_a = v["ka"][...].astype(F32).T
     keys_b = v["kb"][...].astype(F32)
@@ -334,16 +351,16 @@
 
     def along_x(j):
         peer = lax.rem(xx + j, XN)
-        return remote(stack.at[peer], xbox.at[xx], v["xs"].at[j], v["xr"].at[j], {"sp": z * XN + peer})
+        return remote(stack.at[peer], xbox.at[xx], v["xs"], v["xr"], {"sp": z * XN + peer})
 
     def along_z(j):
         peer = lax.rem(z + j, ZN)
         way = jnp.where(peer > z, 0, 1)
-        return remote(agg.at[way], zbox.at[z], v["zs"].at[j], v["zr"].at[j], {"sp": peer * XN + xx})
+        return remote(agg.at[way], zbox.at[z], v["zs"], v["zr"], {"sp": peer * XN + xx})
 
     def back_x(j):
         peer = lax.rem(xx + j, XN)
-        return remote(outx.at[peer], states.at[xx], v["es"].at[j], v["er"].at[j], {"sp": z * XN + peer})
+        return remote(outx.at[peer], states.at[xx], v["es"], v["er"], {"sp": z * XN + peer})
 
     far_x = sorted(range(1, XN), key=lambda j: -near(j, XN))
     far_z = sorted(range(1, ZN), key=lambda j: -near(j, ZN))
@@ -364,9 +381,12 @@
         block = block.astype(F32)
         return block[0:piece], block[piece : piece + 1] + block[piece + 1 : piece + 2]
 
-    for j in range(1, XN):
-        source = lax.rem(xx + XN - j, XN)
-        remote(stack.at[source], xbox.at[source], v["xs"].at[j], v["xr"].at[j], {"sp": z * XN + source}).wait_recv()
+    def all_of(box, size, send, recv):
+        box = box.at[0 : size - 1]
+        return remote(box, box, send, recv, partner)
+
+    if XN > 1:
+        all_of(xbox, XN, v["xs"], v["xr"]).wait_recv()
     for way in range(2):
         state, fade = None, None
         for i in range(XN) if way == 0 else reversed(range(XN)):
@@ -401,9 +421,8 @@
     v["mixhi"][...] = high
     v["mixlo"][...] = (mix - high.astype(F32)).astype(BF16)
 
-    for j in range(1, ZN):
-        source = lax.rem(z + ZN - j, ZN)
-        remote(agg.at[0], zbox.at[source], v["zs"].at[j], v["zr"].at[j], {"sp": source * XN + xx}).wait_recv()
+    if ZN > 1:
+        all_of(zbox, ZN, v["zs"], v["zr"]).wait_recv()
     keys = zbox.shape[2]
     ahead = jnp.zeros((piece, keys), F32)
     behind = jnp.zeros((piece, keys), F32)
@@ -426,11 +445,11 @@
     for j in far_x:
         back_x(j).start()
     states[xx] = outx[xx]
-    for name in ("ga", "gb", "head_gain", "pa", "pb", "stream", "gain_mix", "gain_moe"):
+    for name in ("ga", "gb", "head_gain", "stream", "gain_mix", "gain_moe"):
         fetch[name].wait()
-    for j in range(1, XN):
-        source = lax.rem(xx + XN - j, XN)
-        remote(outx.at[source], states.at[source], v["es"].at[j], v["er"].at[j], {"sp": z * XN + source}).wait_recv()
+    pltpu.make_async_copy(v["pj"].at[0], v["pj"].at[0], v["early"].at[len(order) - 5]).wait()
+    if XN > 1:
+        all_of(states, XN, v["es"], v["er"]).wait_recv()
 
     heads, hbox = v["heads"], v["hbox"]
     for i, (base, dk, gate) in enumerate(((0, DK_A, v["ga"]), (DK_A, DK_B, v["gb"]))):
@@ -462,7 +481,7 @@
     def attn_done(k, total):
         settled[:, k * cut : (k + 1) * cut] = total
 
-    sent = ring_sum(
+    ring_sum(
         y, c, [k // 2 + CUTS // 2 * (k % 2) for k in range(CUTS)], min(2, half), attn_part, lambda o: None,
         lambda: None, v["s1"], v["r1"], v["s1s"], v["s1r"], attn_done,
     )
@@ -477,17 +496,15 @@
     def to_columns(k):
         peer = lax.rem(tp + k, m)
         return remote(
-            moe_in.at[:, lax.rem(peer, YN)], columns.at[:, rows_of(tp), :], v["cs"].at[k], v["cr"].at[k], {"tp": peer}
+            moe_in.at[:, lax.rem(peer, YN)], columns.at[:, rows_of(tp), :], v["cs"], v["cr"], {"tp": peer}
         )
 
     for k in far_tp:
         to_columns(k).start()
     columns[:, rows_of(tp), :] = moe_in[:, lax.rem(tp, YN)]
-    for k in range(1, m):
-        source = lax.rem(tp + m - k, m)
-        remote(
-            moe_in.at[:, 0], columns.at[:, rows_of(source), :], v["cs"].at[k], v["cr"].at[k], {"tp": source}
-        ).wait_recv()
+    most = columns.at[:, 0 : rows - own, :]
+    all_columns = remote(most, most, v["cs"], v["cr"], partner)
+    all_columns.wait_recv()
     wide = mm(v["hot"][...], jnp.concatenate([columns[0], columns[1]], axis=1)).astype(BF16)
     for i in range(2):
         picked[i] = wide[:, i * lanes : (i + 1) * lanes].reshape(n, slots, lanes)
@@ -507,12 +524,12 @@
         j = z_rank[rz] * per + rx // 2
         b = block_of(o)
         return remote(
-            picked.at[b // half, e], seat_of(b, c, j), v["ds"].at[o, dz * XN + dx], v["dr"].at[o, c, j],
+            picked.at[b // half, e], seat_of(b, c, j), v["ds"].at[o, int(dz + dx == 0)], v["dr"].at[groups if o else j // size],
             {"sp": e, "tp": y * 2 + dx % 2},
         )
 
     homes = [
-        pltpu.make_async_copy(picked.at[block_of(o) // half, sp], seat_of(block_of(o), 0, 0), v["dr"].at[o, 0, 0])
+        pltpu.make_async_copy(picked.at[block_of(o) // half, sp], seat_of(block_of(o), 0, 0), v["dr"].at[groups if o else 0])
         for o in range(2)
     ]
     offsets = sorted(
@@ -527,22 +544,20 @@
 
     send_wave(0)
 
-    def arrive(o, j):
-        for k in range(2):
-            coming = remote(
-                picked.at[0, 0], seat_of(block_of(o), k, j), v["ds"].at[0, 0], v["dr"].at[o, k, j], partner
-            )
-            if k == 0 and j == 0:
-                pl.when(c == 0)(lambda: homes[o].wait())
-                pl.when(c == 1)(lambda: coming.wait_recv())
-            else:
-                coming.wait_recv()
+    def arrive(g):
+        block = x.at[block_of(0), g]
+        remote(block, block, v["ds"].at[0, 0], v["dr"].at[g], partner).wait_recv()
+
+    def arrive_opposite():
+        block = x.at[block_of(1)]
+        remote(block, block, v["ds"].at[1, 0], v["dr"].at[groups], partner).wait_recv()
+        widen(block_of(1))
 
     def hop(way, h, g, behind=0):
         step = step_of(way)
         b = lax.rem(y + (h - 1 + behind) * (YN - step), YN)
         return remote(
-            x.at[b, g], x.at[b, g], v["gs"].at[way, h - 1, g], v["gr"].at[way, h - 1, g],
+            x.at[b, g], x.at[b, g], v["gs"], v["gr"].at[h - 1, g],
             {"tp": lax.rem(y + step, YN) * 2 + c},
         )
 
@@ -555,34 +570,37 @@
         value = mm(block, w)
         acc[...] = value if first else acc[...] + value
 
-    for g in range(groups):
-        for j in range(g * size, (g + 1) * size):
-            arrive(0, j)
-        for way in range(2):
-            if half > 1:
-                hop(way, 1, g).start()
-    send_wave(1)
-    for load_w in loads:
-        load_w.wait()
-    for swap in swaps[2:]:
-        swap.wait_recv()
-    widen(y, first=True)
-    for h in range(1, half):
-        if h == half - 1:
-            for j in range(count):
-                arrive(1, j)
-            widen(block_of(1))
-        for g in range(groups):
+    def land(h, g):
+        pair = x.at[0:2, g]
+        remote(pair, pair, v["gs"], v["gr"].at[h - 1, g], partner).wait_recv()
+
+    turns = sorted(
+        [(h, g) for h in range(max(1, half)) for g in range(groups)], key=lambda t: (t[1] + LAG * t[0], t[0])
+    )
+    for h, g in turns:
+        if h == half - 1 and h > 0 and g == 0:
+            arrive_opposite()
+        if h == 0:
+            arrive(g)
+        else:
+            land(h, g)
+        if h < half - 1:
             for way in range(2):
-                hop(way, h, g, 1).wait_recv()
-                if h < half - 1:
-                    hop(way, h + 1, g).start()
-        widen(lax.rem(y + YN - h, YN))
-        widen(lax.rem(y + h, YN))
+                hop(way, h + 1, g).start()
+        if g < groups - 1:
+            continue
+        if h == 0:
+            send_wave(1)
+            for load_w in loads:
+                load_w.wait()
+            for swap in swaps[2:]:
+                swap.wait_recv()
+            widen(y, first=True)
+        else:
+            widen(lax.rem(y + YN - h, YN))
+            widen(lax.rem(y + h, YN))
     if half == 1:
-        for j in range(count):
-            arrive(1, j)
-        widen(block_of(1))
+        arrive_opposite()
 
     hidden = 2 * lanes
     act[...] = (silu(acc[:, :hidden]) * acc[:, hidden:]).astype(BF16)
@@ -595,13 +613,12 @@
     def give(o, k, j):
         rz = z_order[j // per]
         rx = 2 * (j % per) + c
-        back = ((-rz) % ZN) * XN + lax.rem(XN - rx, XN)
         return remote(
-            q.at[o, k, j], pieces.at[o, sp], v["bs"].at[o, k, j], v["br"].at[o, back],
+            q.at[o, k, j], pieces.at[o, sp], v["bs"].at[o, int(k + j == 0)], v["br"].at[o],
             {"sp": sp_at(z, xx, rz, rx), "tp": y * 2 + k},
         )
 
-    returns = [pltpu.make_async_copy(q.at[o, 0, 0], pieces.at[o, sp], v["br"].at[o, 0]) for o in range(2)]
+    returns = [pltpu.make_async_copy(q.at[o, 0, 0], pieces.at[o, sp], v["br"].at[o]) for o in range(2)]
 
     def give_back(o, j):
         for k in range(2):
@@ -628,74 +645,55 @@
         for j in reversed(js):
             give_back(0, j)
 
-    sent += ring_sum(
+    ring_sum(
         y, c, list(reversed(range(groups))), 0, lambda o, g: p[o, g * tall : (g + 1) * tall, :], narrow, opposite,
         v["s2"], v["r2"], v["s2s"], v["s2r"], moe_done,
     )
+    term, mixbox = v["term"], v["mixbox"]
+
+    def spread_rows(o, k):
+        peer = lax.rem(tp + k, m)
+        return remote(term.at[o, rows_of(peer), :], mixbox.at[o, tp], v["fs"].at[o], v["fr"].at[o], {"tp": peer})
+
     for o in (1, 0):
-        for dz in range(ZN):
-            for dx in range(XN):
-                i = dz * XN + dx
-                coming = remote(
-                    q.at[0, 0, 0], pieces.at[o, sp_at(z, xx, dz, dx)], v["bs"].at[0, 0, 0], v["br"].at[o, i], partner
-                )
-                if i == 0:
-                    pl.when(c == 0)(lambda: returns[o].wait())
-                    pl.when(c == 1)(lambda: coming.wait_recv())
-                else:
-                    coming.wait_recv()
-
-    term, mixbox = v["term"], v["mixbox"]
-    flat = jnp.concatenate([pieces[o].reshape(n * slots, lanes) for o in range(2)], axis=1)
-    total = (mm(v["mixhi"][...], flat) + mm(v["mixlo"][...], flat)).astype(BF16)
-    for o in range(2):
-        term[o] = total[:, o * lanes : (o + 1) * lanes]
-
-    def spread_rows(k):
-        peer = lax.rem(tp + k, m)
-        return remote(term.at[:, rows_of(peer), :], mixbox.at[tp], v["fs"].at[k], v["fr"].at[k], {"tp": peer})
-
-    for k in far_tp:
-        spread_rows(k).start()
-    mixbox[tp] = term[:, rows_of(tp), :]
-    for k in range(1, m):
-        source = lax.rem(tp + m - k, m)
-        remote(
-            term.at[:, rows_of(0), :], mixbox.at[source], v["fs"].at[k], v["fr"].at[k], {"tp": source}
-        ).wait_recv()
+        whole = pieces.at[o]
+        remote(whole, whole, v["bs"].at[o, 0], v["br"].at[o], partner).wait_recv()
+        flat = pieces[o].reshape(n * slots, lanes)
+        term[o] = (mm(v["mixhi"][...], flat) + mm(v["mixlo"][...], flat)).astype(BF16)
+        for k in far_tp:
+            spread_rows(o, k).start()
+        mixbox[o, tp] = term[o, rows_of(tp), :]
+    row_waits = []
+    for o in (1, 0):
+        whole = mixbox.at[o, 0 : m - 1]
+        row_waits.append(remote(whole, whole, v["fs"].at[o], v["fr"].at[o], partner))
+        row_waits[-1].wait_recv()
     mixture = jnp.concatenate(
-        [mixbox[i, 0].astype(F32) + mixbox[(i + YN) % m, 1].astype(F32) for i in range(m)], axis=1
+        [mixbox[0, i].astype(F32) + mixbox[1, (i + YN) % m].astype(F32) for i in range(m)], axis=1
     )
     out[...] = layer_norm(settled[...] + mixture, v["gain_moe"][...]).astype(BF16)
 
-    for j in range(1, XN):
-        along_x(j).wait_send()
-        back_x(j).wait_send()
-    for j in range(1, ZN):
-        along_z(j).wait_send()
+    if XN > 1:
+        all_of(xbox, XN, v["xs"], v["xr"]).wait_send()
+        all_of(states, XN, v["es"], v["er"]).wait_send()
+    if ZN > 1:
+        all_of(zbox, ZN, v["zs"], v["zr"]).wait_send()
     hand.wait_send()
     for swap in swaps:
         swap.wait_send()
-    for copy in sent:
-        copy.wait_send()
-    for k in range(1, m):
-        to_columns(k).wait_send()
-        spread_rows(k).wait_send()
+    all_columns.wait_send()
+    for wait in row_waits:
+        wait.wait_send()
     for o in range(2):
-        for dz, dx in offsets:
-            if dz or dx:
-                dispatch(o, dz, dx).wait_send()
+        most = picked.at[0, 0 : n - 1]
+        remote(most, most, v["ds"].at[o, 0], v["dr"].at[o], partner).wait_send()
         pl.when(c == 1)(lambda: dispatch(o, 0, 0).wait_send())
-        for k in range(2):
-            for j in range(count):
-                if k == 0 and j == 0:
-                    pl.when(c == 1)(lambda: give(o, 0, 0).wait_send())
-                else:
-                    give(o, k, j).wait_send()
-    for way in range(2):
-        for h in range(1, half):
-            for g in range(groups):
-                hop(way, h, g).wait_send()
+        most = pieces.at[o, 0 : n - 1]
+        remote(most, most, v["bs"].at[o, 0], v["br"].at[o], partner).wait_send()
+        pl.when(c == 1)(lambda: give(o, 0, 0).wait_send())
+    if half > 1:
+        whole = x.at[0 : 2 * (half - 1)]
+        remote(whole, whole, v["gs"], v["gr"].at[0, 0], partner).wait_send()
 
 
 def body(

time: 105 us -> 98.3 us (0.936)
  Pallas kernels: 104 us -> 96.7 us
    pallas_call x1, Pallas kernels: 104 us -> 96.7 us  [body(): pl.pallas_call(functools.partial(layer_kernel, tuple(scratch)), out_shape...]
where the time goes in v4:
time: 98.3 us; the launch traced here: 98.1 us
  Pallas kernels  96.7 us (98%)
  local copies, waits for them, and re-layouts  1.47 us (1%)
    pallas_call x1, Pallas kernels, body(): pl.pallas_call(functools.partial(layer_kernel, tuple(scratch)), out_shape...  96.7 us

profile of v4, /device:TPU:1, one launch (start us, length us, event | category | flops | bytes accessed | tf_op | source)
XLA Modules:
  0.0 98.1 jit_solution(18274101625114370189)
XLA Ops:
  0.0 96.7 %shard_map.199 = bf16[16,2048]{1,0:T(8,128)(2,1)} custom-call(bf16[64,256]{1,0:T(8,128)(2,1)} %bitcast.9, bf16[64,256]{1,0:T(8,128)(2,1)} %bitcast.10, bf16[256,128]{1,0:T(8,128)(2,1)} %refs_2_.1, bf16[256,128]{1,0:T(8,128)(2,1)} %refs_3_.1, f32[2,64,256]{2,1,0:T(8,128)} %bitcast.8, bf16[256,128]{1,0:T(8,128)(2,1)} %refs_5_.1, bf16[256,128]{1,0:T(8,128)(2,1)} %refs_6_.1, ...), custom_call_target="tpu_custom_call" | custom-call | tf_op jit(solution)/shard_map/pallas_call | solution.py:707
  96.7 1.5 %copy.23 = bf16[16,2048]{1,0:T(8,128)(2,1)} copy(bf16[16,2048]{1,0:T(8,128)(2,1)} %shard_map.199) | data formatting | bytes 131072

commit v5 on v4

--- a/solution.py
+++ b/solution.py
@@ -68,21 +68,26 @@
     return 1 if way == 0 else YN - 1
 
 
-def fade_rows(total):
-    wide = total.shape[1]
-    row = lax.broadcasted_iota(jnp.int32, (FADES, wide), 0)
+def split_fade(total):
     high = total.astype(BF16).astype(F32)
-    return jnp.where(row == 0, high, jnp.where(row == 1, total - high, 0.0)).astype(BF16)
-
-
-def local_states(keys, values, decays, base, stack, cum):
+    return high, total - high
+
+
+def fade_rows(fade_a, fade_b):
+    row = lax.broadcasted_iota(jnp.int32, (FADES, fade_b.shape[1]), 0)
+    rows = 0.0
+    for i, value in enumerate(split_fade(fade_b) + split_fade(fade_a)):
+        rows = jnp.where(row == i, value, rows)
+    return rows.astype(BF16)
+
+
+def local_states(keys, values, decays, base, cum):
     rows, wide = keys.shape
     count = rows // BLK
-    dv = values.shape[1]
-    piece = dv // XN
     ii = lax.broadcasted_iota(jnp.int32, (rows, rows), 0)
     jj = lax.broadcasted_iota(jnp.int32, (rows, rows), 1)
     same = (ii // BLK) == (jj // BLK)
+    found = []
     for way in range(2):
         tri = jnp.where(same & ((ii >= jj) if way == 0 else (ii <= jj)), 1.0, 0.0).astype(BF16)
         fade = log_sigmoid(decays[way]) / SHARPNESS
@@ -97,11 +102,8 @@
             last = part[BLK - 1 : BLK] if way == 0 else part[0:1]
             weighted[b] = (keys[b * BLK : (b + 1) * BLK] * jnp.exp(last - part + tail)).astype(BF16)
             tail = tail + last
-        state = mm_tn(values, jnp.concatenate(weighted, axis=0)).astype(BF16)
-        fades = fade_rows(tail)
-        for i in range(XN):
-            stack[i, way, 0:piece, base : base + wide] = state[i * piece : (i + 1) * piece]
-            stack[i, way, piece : piece + FADES, base : base + wide] = fades
+        found.append((mm_tn(values, jnp.concatenate(weighted, axis=0)).astype(BF16), tail))
+    return found
 
 
 def local_mix(query, keys, values, base, cum, reach, column, mixed):
@@ -187,12 +189,14 @@
         s[way, d - 1, k] = collect(part(d if way == 0 else YN - d, k), way, d, k).astype(BF16)
         pass_sum(way, d, k).start()
 
-    if jump:
-        prepare(half)
-        for k in order:
-            for way in range(2):
-                if mine(way, k):
-                    send(way, half, k)
+    def send_far():
+        if jump:
+            prepare(half)
+            for k in order:
+                for way in range(2):
+                    if mine(way, k):
+                        send(way, half, k)
+
     for d in range(half - 1, 0, -1):
         prepare(d)
         prepare(YN - d)
@@ -201,8 +205,10 @@
             for way in range(2):
                 send(way, d, k)
         if d == half - 1:
+            send_far()
             extra()
     if half == 1:
+        send_far()
         extra()
     prepare(0)
     for k in order:
@@ -235,7 +241,7 @@
     count = n // 2
     group = count * slots
     keys = DK_A + DK_B
-    piece = dv // XN
+    piece = dv // XN + dv // (2 * XN)
     big = piece + FADES
     mine = rows // 2
     groups = min(GROUPS, count)
@@ -250,9 +256,9 @@
         routes=v((2, rows), jnp.int32), affinity=v((2, rows), F32),
         pj=v((2, 2, dv, width), BF16), wg=v((2, width, lanes), BF16), wu=v((2, width, lanes), BF16),
         wd=v((2, lanes, width), BF16), early=DMA((16,)), loads=DMA((3,)), swap_s=DMA((5,)), swap_r=DMA((5,)),
-        cum=v((2, rows, keys), F32), stack=v((XN, 2, big, keys), BF16), xbox=v((XN, 2, big, keys), BF16),
-        agg=v((2, big, keys), BF16), zbox=v((ZN, big, keys), BF16), outx=v((XN, 2, piece, keys), BF16),
-        states=v((XN, 2, piece, keys), BF16), xs=DMA, xr=DMA, zs=DMA, zr=DMA,
+        cum=v((2, rows, keys), F32), stack=v((XN, 2, big, DK_B), BF16), xbox=v((XN, 2, big, DK_B), BF16),
+        agg=v((2, big, DK_B), BF16), zbox=v((ZN, big, DK_B), BF16), outx=v((XN, 2, piece, DK_B), BF16),
+        states=v((XN, 2, piece, DK_B), BF16), xs=DMA, xr=DMA, zs=DMA, zr=DMA,
         es=DMA, er=DMA,
         mixed=v((rows, 2 * dv), F32), reach=v((2, rows, keys), BF16), heads=v((2, mine, 2 * dv), BF16),
         hbox=v((mine, 2 * dv), BF16), hs=DMA((2,)), pp=v((YN, own, width), F32),
@@ -341,13 +347,23 @@
     cum, stack = v["cum"], v["stack"]
     keys_a = v["ka"][...].astype(F32).T
     keys_b = v["kb"][...].astype(F32)
-    local_states(keys_a, v["va"][...], [v["da"][i].T for i in range(2)], 0, stack, cum)
-    local_states(keys_b, v["vb"][...], [v["db"][i] for i in range(2)], DK_A, stack, cum)
+    found_b = local_states(keys_b, v["vb"][...], [v["db"][i] for i in range(2)], 0, cum)
+    found_a = local_states(keys_a, v["va"][...], [v["da"][i].T for i in range(2)], DK_B, cum)
+    dv = v["va"].shape[1]
+    tall_b, tall_a = dv // XN, dv // (2 * XN)
+    piece = tall_b + tall_a
+    for way in range(2):
+        (state_a, fade_a), (state_b, fade_b) = found_a[way], found_b[way]
+        state_a = jnp.concatenate([state_a[0 : dv // 2], state_a[dv // 2 : dv]], axis=1)
+        fades = fade_rows(jnp.concatenate([fade_a, fade_a], axis=1), fade_b)
+        for i in range(XN):
+            stack[i, way, 0:tall_b] = state_b[i * tall_b : (i + 1) * tall_b]
+            stack[i, way, tall_b:piece] = state_a[i * tall_a : (i + 1) * tall_a]
+            stack[i, way, piece : piece + FADES] = fades
 
     pl.semaphore_wait(barrier, greeted)
 
     xbox, agg, zbox, outx, states = (v[i] for i in ("xbox", "agg", "zbox", "outx", "states"))
-    piece = outx.shape[2]
 
     def along_x(j):
         peer = lax.rem(xx + j, XN)
@@ -374,12 +390,20 @@
     for name in ("qa", "qb"):
         fetch[name].wait()
     mixed, reach = v["mixed"], v["reach"]
-    dv = v["va"].shape[1]
-    local_mix(v["qa"][...].astype(F32).T, keys_a, v["va"][...], 0, cum, reach, 0, mixed)
+    local_mix(v["qa"][...].astype(F32).T, keys_a, v["va"][...], DK_B, cum, reach, 0, mixed)
 
     def load(block):
         block = block.astype(F32)
-        return block[0:piece], block[piece : piece + 1] + block[piece + 1 : piece + 2]
+        fades = block[piece : piece + FADES]
+        return (block[0:tall_b], block[tall_b:piece]), (fades[0:1] + fades[1:2], fades[2:3] + fades[3:4])
+
+    def advance(state, block):
+        own, fade = load(block)
+        return tuple(jnp.exp(f) * s + o for f, s, o in zip(fade, state, own))
+
+    def keep(ref, at, state):
+        ref[at + (slice(0, tall_b),)] = state[0].astype(BF16)
+        ref[at + (slice(tall_b, piece),)] = state[1].astype(BF16)
 
     def all_of(box, size, send, recv):
         box = box.at[0 : size - 1]
@@ -388,17 +412,17 @@
     if XN > 1:
         all_of(xbox, XN, v["xs"], v["xr"]).wait_recv()
     for way in range(2):
-        state, fade = None, None
+        state, fades = None, None
         for i in range(XN) if way == 0 else reversed(range(XN)):
             own_state, own_fade = load(xbox[i, way])
-            state = own_state if state is None else jnp.exp(own_fade) * state + own_state
-            fade = own_fade if fade is None else fade + own_fade
-        agg[way, 0:piece] = state.astype(BF16)
-        agg[way, piece : piece + FADES] = fade_rows(fade)
+            state = own_state if state is None else advance(state, xbox[i, way])
+            fades = own_fade if fades is None else tuple(a + b for a, b in zip(fades, own_fade))
+        keep(agg, (way,), state)
+        agg[way, piece : piece + FADES] = fade_rows(fades[1], fades[0])
     for j in far_z:
         along_z(j).start()
 
-    local_mix(v["qb"][...].astype(F32), keys_b, v["vb"][...], DK_A, cum, reach, dv, mixed)
+    local_mix(v["qb"][...].astype(F32), keys_b, v["vb"][...], 0, cum, reach, dv, mixed)
     for name in ("routes", "affinity"):
         fetch[name].wait()
     routes, affinity = v["routes"][...], v["affinity"][...]
@@ -423,25 +447,20 @@
 
     if ZN > 1:
         all_of(zbox, ZN, v["zs"], v["zr"]).wait_recv()
-    keys = zbox.shape[2]
-    ahead = jnp.zeros((piece, keys), F32)
-    behind = jnp.zeros((piece, keys), F32)
+    start = tuple(jnp.zeros((tall, zbox.shape[2]), F32) for tall in (tall_b, tall_a))
+    ahead, behind = start, start
     for i in range(ZN):
-        state, fade = load(zbox[i])
-        ahead = jnp.where(i < z, jnp.exp(fade) * ahead + state, ahead)
+        ahead = tuple(jnp.where(i < z, a, b) for a, b in zip(advance(ahead, zbox[i]), ahead))
     for i in reversed(range(ZN)):
-        state, fade = load(zbox[i])
-        behind = jnp.where(i > z, jnp.exp(fade) * behind + state, behind)
+        behind = tuple(jnp.where(i > z, a, b) for a, b in zip(advance(behind, zbox[i]), behind))
     for i in range(XN):
-        outx[i, 0] = ahead.astype(BF16)
+        keep(outx, (i, 0), ahead)
         if i < XN - 1:
-            state, fade = load(xbox[i, 0])
-            ahead = jnp.exp(fade) * ahead + state
+            ahead = advance(ahead, xbox[i, 0])
     for i in reversed(range(XN)):
-        outx[i, 1] = behind.astype(BF16)
+        keep(outx, (i, 1), behind)
         if i > 0:
-            state, fade = load(xbox[i, 1])
-            behind = jnp.exp(fade) * behind + state
+            behind = advance(behind, xbox[i, 1])
     for j in far_x:
         back_x(j).start()
     states[xx] = outx[xx]
@@ -452,12 +471,15 @@
         all_of(states, XN, v["es"], v["er"]).wait_recv()
 
     heads, hbox = v["heads"], v["hbox"]
-    for i, (base, dk, gate) in enumerate(((0, DK_A, v["ga"]), (DK_A, DK_B, v["gb"]))):
-        at = slice(base, base + dk)
+    for i, (base, dk, gate) in enumerate(((DK_B, DK_A, v["ga"]), (0, DK_B, v["gb"]))):
         whole = mixed[:, i * dv : (i + 1) * dv]
         for way in range(2):
-            start = states[:, way].reshape(dv, keys)
-            whole = whole + mm_nt(reach[way, :, at], start[:, at])
+            if i == 0:
+                start = states[:, way, tall_b:piece].reshape(dv // 2, 2 * DK_A)
+                start = jnp.concatenate([start[:, 0:DK_A], start[:, DK_A:]], axis=0)
+            else:
+                start = states[:, way, 0:tall_b].reshape(dv, DK_B)
+            whole = whole + mm_nt(reach[way, :, base : base + dk], start)
         scale = lax.rsqrt(jnp.mean(whole * whole, axis=-1, keepdims=True) + 1e-06)
         value = (whole * scale * v["head_gain"][...] * silu(gate[...].astype(F32))).astype(BF16)
         value = value.reshape(YN, 2, own, dv)
@@ -482,7 +504,7 @@
         settled[:, k * cut : (k + 1) * cut] = total
 
     ring_sum(
-        y, c, [k // 2 + CUTS // 2 * (k % 2) for k in range(CUTS)], min(2, half), attn_part, lambda o: None,
+        y, c, [k // 2 + CUTS // 2 * (k % 2) for k in range(CUTS)], min(3, half), attn_part, lambda o: None,
         lambda: None, v["s1"], v["r1"], v["s1s"], v["s1r"], attn_done,
     )
     value = layer_norm(v["stream"][...].astype(F32) + settled[...], v["gain_mix"][...])
@@ -533,7 +555,7 @@
         for o in range(2)
     ]
     offsets = sorted(
-        [(dz, dx) for dz in range(ZN) for dx in range(XN)], key=lambda o: near(o[0], ZN) + near(o[1], XN)
+        [(dz, dx) for dz in range(ZN) for dx in range(XN)], key=lambda o: (z_rank[-o[0] % ZN], -near(o[1], XN))
     )
     def send_wave(o):
         for dz, dx in offsets:

time: 98.3 us -> 95.7 us (0.974)
  Pallas kernels: 96.7 us -> 94 us
    pallas_call x1, Pallas kernels: 96.7 us -> 94 us  [body(): pl.pallas_call(functools.partial(layer_kernel, tuple(scratch)), out_shape...]
where the time goes in v5:
time: 95.7 us; the launch traced here: 95.5 us
  Pallas kernels  94 us (98%)
  local copies, waits for them, and re-layouts  1.47 us (2%)
    pallas_call x1, Pallas kernels, body(): pl.pallas_call(functools.partial(layer_kernel, tuple(scratch)), out_shape...  94 us

profile of v5, /device:TPU:1, one launch (start us, length us, event | category | flops | bytes accessed | tf_op | source)
XLA Modules:
  0.0 95.5 jit_solution(5672791515158963194)
XLA Ops:
  0.0 94.0 %shard_map.199 = bf16[16,2048]{1,0:T(8,128)(2,1)} custom-call(bf16[64,256]{1,0:T(8,128)(2,1)} %bitcast.9, bf16[64,256]{1,0:T(8,128)(2,1)} %bitcast.10, bf16[256,128]{1,0:T(8,128)(2,1)} %refs_2_.1, bf16[256,128]{1,0:T(8,128)(2,1)} %refs_3_.1, f32[2,64,256]{2,1,0:T(8,128)} %bitcast.8, bf16[256,128]{1,0:T(8,128)(2,1)} %refs_5_.1, bf16[256,128]{1,0:T(8,128)(2,1)} %refs_6_.1, ...), custom_call_target="tpu_custom_call" | custom-call | tf_op jit(solution)/shard_map/pallas_call | solution.py:729
  94.0 1.5 %copy.23 = bf16[16,2048]{1,0:T(8,128)(2,1)} copy(bf16[16,2048]{1,0:T(8,128)(2,1)} %shard_map.199) | data formatting | bytes 131072

commit v6 on v5

--- a/solution.py
+++ b/solution.py
@@ -260,7 +260,7 @@
         agg=v((2, big, DK_B), BF16), zbox=v((ZN, big, DK_B), BF16), outx=v((XN, 2, piece, DK_B), BF16),
         states=v((XN, 2, piece, DK_B), BF16), xs=DMA, xr=DMA, zs=DMA, zr=DMA,
         es=DMA, er=DMA,
-        mixed=v((rows, 2 * dv), F32), reach=v((2, rows, keys), BF16), heads=v((2, mine, 2 * dv), BF16),
+        mixed=v((rows, 2 * dv), F32), shine=v((rows, 2 * dv), F32), reach=v((2, rows, keys), BF16), heads=v((2, mine, 2 * dv), BF16),
         hbox=v((mine, 2 * dv), BF16), hs=DMA((2,)), pp=v((YN, own, width), F32),
         s1=v((2, half, CUTS, own, cut), BF16), r1=v((2, half, CUTS, own, cut), BF16),
         s1s=DMA((2,)), s1r=DMA((half, CUTS)), settled=v((own, width), F32),
@@ -318,8 +318,8 @@
         return near(dz, ZN) + near(dx, XN) + near(dy, YN)
 
     friends = [
-        (far(dz, dx, 0), {"sp": sp_at(z, xx, dz, dx), "tp": y * 2 + core})
-        for dz in range(ZN) for dx in range(XN) for core in range(2) if dz or dx
+        (far(dz, dx, 0), {"sp": sp_at(z, xx, dz, dx)})
+        for dz in range(ZN) for dx in range(XN) if (dz == 0) != (dx == 0)
     ] + [(far(0, 0, k // 2), {"tp": lax.rem(tp + k, m)}) for k in range(1, m)]
     for _, peer in sorted(friends, key=lambda f: -f[0]):
         pl.semaphore_signal(barrier, inc=1, device_id=peer, device_id_type=MESH)
@@ -423,8 +423,10 @@
         along_z(j).start()
 
     local_mix(v["qb"][...].astype(F32), keys_b, v["vb"][...], 0, cum, reach, dv, mixed)
-    for name in ("routes", "affinity"):
+    for name in ("routes", "affinity", "ga", "gb", "head_gain"):
         fetch[name].wait()
+    for i, gate in enumerate((v["ga"], v["gb"])):
+        v["shine"][:, i * dv : (i + 1) * dv] = v["head_gain"][...] * silu(gate[...].astype(F32))
     routes, affinity = v["routes"][...], v["affinity"][...]
     lane = lax.broadcasted_iota(jnp.int32, (n, rows), 0)
     hots = [routes[i : i + 1] == lane for i in range(2)]
@@ -464,14 +466,14 @@
     for j in far_x:
         back_x(j).start()
     states[xx] = outx[xx]
-    for name in ("ga", "gb", "head_gain", "stream", "gain_mix", "gain_moe"):
+    for name in ("stream", "gain_mix", "gain_moe"):
         fetch[name].wait()
     pltpu.make_async_copy(v["pj"].at[0], v["pj"].at[0], v["early"].at[len(order) - 5]).wait()
     if XN > 1:
         all_of(states, XN, v["es"], v["er"]).wait_recv()
 
     heads, hbox = v["heads"], v["hbox"]
-    for i, (base, dk, gate) in enumerate(((DK_B, DK_A, v["ga"]), (0, DK_B, v["gb"]))):
+    for i, (base, dk) in enumerate(((DK_B, DK_A), (0, DK_B))):
         whole = mixed[:, i * dv : (i + 1) * dv]
         for way in range(2):
             if i == 0:
@@ -481,7 +483,7 @@
                 start = states[:, way, 0:tall_b].reshape(dv, DK_B)
             whole = whole + mm_nt(reach[way, :, base : base + dk], start)
         scale = lax.rsqrt(jnp.mean(whole * whole, axis=-1, keepdims=True) + 1e-06)
-        value = (whole * scale * v["head_gain"][...] * silu(gate[...].astype(F32))).astype(BF16)
+        value = (whole * scale * v["shine"][:, i * dv : (i + 1) * dv]).astype(BF16)
         value = value.reshape(YN, 2, own, dv)
         for core in range(2):
             heads[core, :, i * dv : (i + 1) * dv] = value[:, core].reshape(YN * own, dv)
@@ -527,9 +529,12 @@
     most = columns.at[:, 0 : rows - own, :]
     all_columns = remote(most, most, v["cs"], v["cr"], partner)
     all_columns.wait_recv()
-    wide = mm(v["hot"][...], jnp.concatenate([columns[0], columns[1]], axis=1)).astype(BF16)
-    for i in range(2):
-        picked[i] = wide[:, i * lanes : (i + 1) * lanes].reshape(n, slots, lanes)
+
+    def pick(o):
+        i = lax.rem(y + o * half, YN) // half
+        picked[i] = mm(v["hot"][...], columns[i]).astype(BF16).reshape(n, slots, lanes)
+
+    pick(0)
 
     z_order = sorted(range(ZN), key=lambda d: near(d, ZN))
     z_rank = [z_order.index(d) for d in range(ZN)]
@@ -565,6 +570,7 @@
         pl.when(c == 1)(lambda: dispatch(o, 0, 0).start())
 
     send_wave(0)
+    pick(1)
 
     def arrive(g):
         block = x.at[block_of(0), g]
@@ -585,12 +591,16 @@
 
     wg, wu, wd = v["wg"], v["wu"], v["wd"]
 
-    def widen(b, first=False):
+    def widen(b, first=False, low=0, high=groups):
+        tall = group // groups
+        span = slice(low * tall, high * tall)
         at = pl.ds(pl.multiple_of(b * 2 * lanes, 2 * lanes), 2 * lanes)
-        block = jnp.concatenate([x[b, :, k].reshape(group, lanes) for k in range(2)], axis=1)
+        block = jnp.concatenate(
+            [x[b, low:high, k].reshape((high - low) * tall, lanes) for k in range(2)], axis=1
+        )
         w = jnp.concatenate([ref[i, at, :] for ref in (wg, wu) for i in range(2)], axis=1)
         value = mm(block, w)
-        acc[...] = value if first else acc[...] + value
+        acc[span] = value if first else acc[span] + value
 
     def land(h, g):
         pair = x.at[0:2, g]
@@ -609,7 +619,8 @@
         if h < half - 1:
             for way in range(2):
                 hop(way, h + 1, g).start()
-        if g < groups - 1:
+        cut_at = groups // 2 if h == half - 1 and h > 0 else 0
+        if g < groups - 1 and g + 1 != cut_at:
             continue
         if h == 0:
             send_wave(1)
@@ -619,8 +630,9 @@
                 swap.wait_recv()
             widen(y, first=True)
         else:
-            widen(lax.rem(y + YN - h, YN))
-            widen(lax.rem(y + h, YN))
+            edges = (0, cut_at) if g + 1 == cut_at else (cut_at, groups)
+            widen(lax.rem(y + YN - h, YN), False, *edges)
+            widen(lax.rem(y + h, YN), False, *edges)
     if half == 1:
         arrive_opposite()
 

time: 95.7 us -> 95.4 us (level)
  no operation moved by 1% of the time
where the time goes in v6:
time: 95.4 us; the launch traced here: 95.2 us
  Pallas kernels  93.8 us (98%)
  local copies, waits for them, and re-layouts  1.47 us (2%)
    pallas_call x1, Pallas kernels, body(): pl.pallas_call(functools.partial(layer_kernel, tuple(scratch)), out_shape...  93.8 us

profile of v6, /device:TPU:1, one launch (start us, length us, event | category | flops | bytes accessed | tf_op | source)
XLA Modules:
  0.0 95.2 jit_solution(13615031225732017890)
XLA Ops:
  0.0 93.8 %shard_map.199 = bf16[16,2048]{1,0:T(8,128)(2,1)} custom-call(bf16[64,256]{1,0:T(8,128)(2,1)} %bitcast.9, bf16[64,256]{1,0:T(8,128)(2,1)} %bitcast.10, bf16[256,128]{1,0:T(8,128)(2,1)} %refs_2_.1, bf16[256,128]{1,0:T(8,128)(2,1)} %refs_3_.1, f32[2,64,256]{2,1,0:T(8,128)} %bitcast.8, bf16[256,128]{1,0:T(8,128)(2,1)} %refs_5_.1, bf16[256,128]{1,0:T(8,128)(2,1)} %refs_6_.1, ...), custom_call_target="tpu_custom_call" | custom-call | tf_op jit(solution)/shard_map/pallas_call | solution.py:741
  93.8 1.5 %copy.23 = bf16[16,2048]{1,0:T(8,128)(2,1)} copy(bf16[16,2048]{1,0:T(8,128)(2,1)} %shard_map.199) | data formatting | bytes 131072
